TPU v7x, 32 devices: a whole 2x2x4 slice. The times are simulated.
32 devices in a mesh: kv: 8 (over z, x), tp: 4 (over y, core).
Axes of the slice: x: 2, y: 2, z: 4, core: 2. Of those that a mesh axis runs over, the one named last changes fastest.
Arguments:
- inputs: bfloat16 [4, 2048, 2048], P(None, 'kv'), may hold values from -40 to 40
- query_weight: bfloat16 [2048, 2048], P(None, 'tp'), may hold values from -0.125 to 0.125
- key_weight: bfloat16 [2048, 1024], P(None, 'tp'), may hold values from -0.125 to 0.125
- value_weight: bfloat16 [2048, 1024], P(None, 'tp'), may hold values from -0.125 to 0.125
- out_weight: bfloat16 [2048, 2048], P('tp'), may hold values from -1 to 1
- chosen: int32 [4, 32, 32], P(None, 'kv'), may hold values from 0 to 31, as said below
- lengths: int32 [4], replicated, may hold values from 1 to 2048, 3072 in all
Outputs:
- mixed: bfloat16 [4, 2048, 2048], P(None, 'kv', 'tp')
Inputs may be any that keep to these rules, and one draw needn't show every extreme that they name: chosen[b, q, 0] = q; every entry names a block of the same sequence at or before q; entries may repeat. Over the query blocks of positions k * 256 to (k+1) * 256 - 1 of all sequences, the named blocks that lie in another span of 256 positions number at most 3 distinct blocks for each other span, and 3 is reached.
All inputs are finite; a program needn't handle non-finite values.
Results may differ from a plain program's by a relative error of at most 0.014.
The roundings to bfloat16 on the way count: a program that leaves them out, or rounds other values in their place, can miss the bound.
Values may be sent and summed in bfloat16 or wider, within the bound.
A program may use at most 128 MiB of HBM per device.

v0:
```python
import functools

import jax
import jax.numpy as jnp
from jax import lax
from jax.experimental import pallas as pl
from jax.experimental.pallas import tpu as pltpu
from jax.sharding import PartitionSpec as P

HD = 128
KB = 64
CAP = 3
MASKED = -1e30


def tables(chosen, devices, device):
    batch_size, per_dev, _ = chosen.shape
    blocks = jnp.arange(devices * per_dev, dtype=jnp.int32)
    named = jnp.any(chosen[..., None] == blocks, axis=2)
    named = named.reshape(batch_size, per_dev, devices, per_dev)
    own = jnp.sum(
        jnp.where(jnp.arange(devices)[None, None, :, None] == device, named, False), axis=2
    )
    needed = jnp.any(named, axis=1) & (jnp.arange(devices)[None, :, None] != device)
    needed = jnp.transpose(needed, (1, 0, 2)).reshape(devices, batch_size * per_dev)
    local = jnp.arange(batch_size * per_dev, dtype=jnp.int32)
    slots = jnp.sum(
        jnp.where(local[None, :, None] > local[None, None, :], needed[:, None, :], False),
        axis=2,
        dtype=jnp.int32,
    )
    matches = needed[:, :, None] & (slots[:, :, None] == jnp.arange(CAP, dtype=jnp.int32))
    requests = jnp.sum(jnp.where(matches, local[None, :, None], 0), axis=1)
    matches = matches.reshape(devices, batch_size, per_dev, CAP)
    matches = jnp.transpose(matches, (1, 0, 2, 3))
    remote = jnp.any(named[..., None] & matches[:, None], axis=3)
    own_bias = jnp.where(own > 0, 0.0, MASKED).astype(jnp.float32)
    own_bias = jnp.repeat(own_bias, KB, axis=-1)
    home = device * per_dev + jnp.arange(per_dev, dtype=jnp.int32)
    copies = jnp.sum(chosen == home[None, :, None], axis=-1, dtype=jnp.int32)
    same = jnp.log(jnp.maximum(copies, 1).astype(jnp.float32))
    same = jnp.broadcast_to(same[..., None], own_bias.shape)
    rem_bias = jnp.where(remote, 0.0, MASKED).astype(jnp.float32)
    rem_bias = rem_bias.reshape(batch_size, per_dev, devices // 2, 2 * CAP)
    rem_bias = jnp.repeat(jnp.transpose(rem_bias, (2, 0, 1, 3)), KB, axis=-1)
    return requests, jnp.stack([own_bias, same]), rem_bias


def attend_kernel(
    positions, kv_local, per_group, length_ref, q_ref, k_ref, v_ref, rem_ref,
    own_bias_ref, rem_bias_ref, out_ref, scores_ref
):
    device = lax.axis_index("kv")
    batch_size = own_bias_ref.shape[1]
    per_dev = positions // KB
    wide = rem_bias_ref.shape[-1]
    rows = per_group * positions
    chunks = (device + 1) // 2
    scaling = HD ** (-0.5)
    contract = (((1,), (1,)), ((), ()))

    def masked(scores, bias):
        width = scores.shape[-1]
        shaped = (scores * scaling).reshape(per_group, per_dev, KB, width)
        return (shaped + bias[None, :, None, :]).reshape(rows, width)

    @pl.loop(0, batch_size)
    def _(b):
        live = length_ref[b] - device * positions
        here = pl.ds(pl.multiple_of(b * positions, positions), positions)

        @pl.when(live <= 0)
        def _():
            out_ref[here, :] = jnp.zeros((positions, out_ref.shape[1]), out_ref.dtype)

        @pl.when(live > 0)
        def _():
            at_row = lax.broadcasted_iota(jnp.int32, (positions, positions), 0)
            at_col = lax.broadcasted_iota(jnp.int32, (positions, positions), 1)
            before, same = [
                jnp.broadcast_to(own_bias_ref[i, b][:, None, :], (per_dev, KB, positions)).reshape(
                    positions, positions
                )
                for i in range(2)
            ]
            own_bias = jnp.where(
                at_col < at_row, before, jnp.where(at_col == at_row, same, MASKED)
            )
            living = lax.broadcasted_iota(jnp.int32, (positions, HD), 0) < live
            for h in range(kv_local):
                cols = slice(h * HD, (h + 1) * HD)
                far_cols = slice((kv_local + h) * HD, (kv_local + h + 1) * HD)
                heads = [h * per_group + g for g in range(per_group)]
                queries = jnp.concatenate(
                    [q_ref[here, n * HD:(n + 1) * HD] for n in heads], axis=0
                )
                own = lax.dot_general(
                    queries, k_ref[here, cols], contract, preferred_element_type=jnp.float32
                )
                own = (own * scaling).reshape(per_group, positions, positions) + own_bias[None]
                own = own.reshape(rows, positions)
                top = jnp.max(own, axis=-1, keepdims=True)

                def score(c, top):
                    there = pl.ds(pl.multiple_of(c * wide, wide), wide)
                    far = lax.dot_general(
                        queries, rem_ref[there, cols], contract,
                        preferred_element_type=jnp.float32,
                    )
                    far = masked(far, rem_bias_ref[c, b])
                    scores_ref[c] = far
                    return jnp.maximum(top, jnp.max(far, axis=-1, keepdims=True))

                top = lax.fori_loop(0, chunks, score, top)
                raised = jnp.exp(own - top)
                total = jnp.sum(raised, axis=-1, keepdims=True)
                mixed = jnp.dot(
                    raised.astype(jnp.bfloat16), v_ref[here, cols],
                    preferred_element_type=jnp.float32,
                )

                def gather(c, carry):
                    total, mixed = carry
                    there = pl.ds(pl.multiple_of(c * wide, wide), wide)
                    raised = jnp.exp(scores_ref[c] - top)
                    total = total + jnp.sum(raised, axis=-1, keepdims=True)
                    mixed = mixed + jnp.dot(
                        raised.astype(jnp.bfloat16), rem_ref[there, far_cols],
                        preferred_element_type=jnp.float32,
                    )
                    return total, mixed

                total, mixed = lax.fori_loop(0, chunks, gather, (total, mixed))
                mixed = mixed / total
                for g, n in enumerate(heads):
                    part = mixed[g * positions:(g + 1) * positions]
                    out_ref[here, n * HD:(n + 1) * HD] = jnp.where(living, part, 0.0).astype(
                        out_ref.dtype
                    )


def attend(positions, kv_local, per_group, lengths, queries, k, v, rem, own_bias, rem_bias):
    vmem = pl.BlockSpec(memory_space=pltpu.VMEM)
    return pl.pallas_call(
        functools.partial(attend_kernel, positions, kv_local, per_group),
        out_shape=jax.ShapeDtypeStruct(queries.shape, jnp.bfloat16),
        in_specs=[pl.BlockSpec(memory_space=pltpu.SMEM)] + [vmem] * 6,
        out_specs=vmem,
        scratch_shapes=[
            pltpu.VMEM(
                (rem_bias.shape[0], per_group * positions, rem_bias.shape[-1]), jnp.float32
            )
        ],
        compiler_params=pltpu.CompilerParams(vmem_limit_bytes=48 * 2**20),
    )(lengths, queries, k, v, rem, own_bias, rem_bias)


def mix_kernel(
    steps, tp, att_ref, weight_ref, out_ref,
    pair_out, pair_in, far_out, far_in, near,
    pair_sent, pair_got, far_sent, far_got,
):
    me = lax.axis_index("tp")
    core = lax.rem(me, 2)
    chip = me // 2
    chips = tp // 2
    partner = me + 1 - 2 * core
    width = out_ref.shape[1]
    step_rows = out_ref.shape[0] // steps
    mesh_id = pl.DeviceIdType.MESH

    def twin(off):
        return lax.rem(chip + off, chips) * 2 + core

    barrier = pltpu.get_barrier_semaphore()
    pl.semaphore_signal(barrier, inc=1, device_id={"tp": partner}, device_id_type=mesh_id)
    for off in range(1, chips):
        pl.semaphore_signal(barrier, inc=1, device_id={"tp": twin(off)}, device_id_type=mesh_id)
    pl.semaphore_wait(barrier, chips)

    def at(i):
        return pl.ds(pl.multiple_of(i * step_rows, step_rows), step_rows)

    def group_sum(i, off, side):
        column = (lax.rem(chip + off, chips) * 2 + side) * width
        return jnp.dot(
            att_ref[at(i), :],
            weight_ref[:, pl.ds(pl.multiple_of(column, width), width)],
            preferred_element_type=jnp.float32,
        ).astype(jnp.bfloat16)

    def pair_copy(i):
        return pltpu.make_async_remote_copy(
            src_ref=pair_out.at[i], dst_ref=pair_in.at[i],
            send_sem=pair_sent.at[i], recv_sem=pair_got.at[i],
            device_id={"tp": partner}, device_id_type=mesh_id,
        )

    def far_copy(i, off):
        return pltpu.make_async_remote_copy(
            src_ref=far_out.at[off - 1, i], dst_ref=far_in.at[off - 1, i],
            send_sem=far_sent.at[off - 1, i], recv_sem=far_got.at[off - 1, i],
            device_id={"tp": twin(off)}, device_id_type=mesh_id,
        )

    def step(i, carry):
        @pl.when(i < steps)
        def _():
            for off in range(chips):
                pair_out[i, off] = group_sum(i, off, 1 - core)
            pair_copy(i).start()

        @pl.when(i > 0)
        def _():
            j = i - 1
            sums = [group_sum(j, off, core).astype(jnp.float32) for off in range(chips)]
            pair_copy(j).wait_recv()
            for off in range(1, chips):
                both = sums[off] + pair_in[j, off].astype(jnp.float32)
                far_out[off - 1, j] = both.astype(jnp.bfloat16)
                far_copy(j, off).start()
            near[j] = sums[0] + pair_in[j, 0].astype(jnp.float32)

        return carry

    lax.fori_loop(0, steps + 1, step, 0)

    def finish(i, carry):
        pair_copy(i).wait_send()
        mixed = near[i]
        for off in range(1, chips):
            far_copy(i, off).wait()
            mixed = mixed + far_in[off - 1, i].astype(jnp.float32)
        out_ref[at(i), :] = mixed.astype(out_ref.dtype)
        return carry

    lax.fori_loop(0, steps, finish, 0)


def mix(attended, out_weight, tp):
    rows = attended.shape[0]
    width = out_weight.shape[1] // tp
    chips = tp // 2
    steps = rows // 128
    vmem = pl.BlockSpec(memory_space=pltpu.VMEM)
    pair = pltpu.VMEM((steps, chips, rows // steps, width), jnp.bfloat16)
    far = pltpu.VMEM((chips - 1, steps, rows // steps, width), jnp.bfloat16)
    return pl.pallas_call(
        functools.partial(mix_kernel, steps, tp),
        out_shape=jax.ShapeDtypeStruct((rows, width), jnp.bfloat16),
        in_specs=[vmem, vmem],
        out_specs=vmem,
        scratch_shapes=[
            pair, pair, far, far,
            pltpu.VMEM((steps, rows // steps, width), jnp.float32),
            pltpu.SemaphoreType.DMA((steps,)),
            pltpu.SemaphoreType.DMA((steps,)),
            pltpu.SemaphoreType.DMA((chips - 1, steps)),
            pltpu.SemaphoreType.DMA((chips - 1, steps)),
        ],
        compiler_params=pltpu.CompilerParams(
            collective_id=0, has_side_effects=True, vmem_limit_bytes=48 * 2**20
        ),
    )(attended, out_weight)


def shards(inputs, query_weight, key_weight, value_weight, out_weight, chosen, lengths):
    batch_size, positions, model_width = inputs.shape
    kv_local = key_weight.shape[1] // HD
    heads_local = query_weight.shape[1] // HD
    per_group = heads_local // kv_local
    owned = batch_size * (positions // KB)
    device = lax.axis_index("kv")
    devices = lax.axis_size("kv")
    flat_rows = inputs.reshape(batch_size * positions, model_width)

    def project(weight):
        return jnp.dot(flat_rows, weight, preferred_element_type=jnp.float32).astype(jnp.bfloat16)

    queries = project(query_weight)
    key_rows = project(key_weight)
    value_rows = project(value_weight)
    requests, own_bias, rem_bias = tables(chosen, devices, device)
    asked = lax.all_to_all(requests, "kv", split_axis=0, concat_axis=0, tiled=True)

    picked = jnp.concatenate(
        [
            table.reshape(owned, KB, kv_local * HD)[asked]
            for table in (key_rows, value_rows)
        ],
        axis=-1,
    )
    got = lax.all_to_all(picked, "kv", split_axis=0, concat_axis=0, tiled=True)
    got = got.reshape(devices * CAP * KB, 2 * kv_local * HD)
    attended = attend(
        positions, kv_local, per_group, lengths, queries, key_rows, value_rows,
        got, own_bias, rem_bias,
    )
    mixed = mix(attended, out_weight, lax.axis_size("tp"))
    return mixed.reshape(batch_size, positions, -1)


def solution(mesh):
    placed = (
        P(None, "kv", None),
        P(None, "tp"),
        P(None, "tp"),
        P(None, "tp"),
        P("tp", None),
        P(None, "kv", None),
        P(),
    )
    return jax.shard_map(
        shards, mesh=mesh, in_specs=placed, out_specs=P(None, "kv", "tp"), check_vma=False
    )
```

profile of v0, /device:TPU:0, one launch (start us, length us, event | category | flops | bytes accessed | tf_op | source)
XLA Modules:
  0.0 100.0 jit_solution(1616549767664905131)
XLA Ops:
  0.0 1.0 %fusion = (pred[4,4,32]{2,1,0:T(4,128)(4,1)S(1)}, pred[4,32]{1,0:T(4,128)(4,1)S(1)}) fusion(s32[4,4,32]{2,1,0:T(4,128)} %param.12), kind=kLoop, calls=%fused_computation.7 | loop fusion | flops 48512 | bytes 2688 | tf_op jit(solution)/shard_map/reduce_or | solution.py:19
  1.0 0.1 reduce_or.30
  1.2 0.1 copy.30
  1.3 0.1 copy.31
  1.4 0.2 convert_reduce_fusion.1
  1.6 0.1 select_reduce_fusion
  1.8 0.7 copy.33
  2.5 7.3 %all-to-all-start = ((s32[8,1,3]{2,1,0:T(1,128)}), s32[8,1,3]{2,1,0:T(1,128)S(1)}, u32[]{:S(2)}, u32[]{:S(2)}) async-start(s32[8,1,3]{2,1,0:T(1,128)} %copy.33), calls=%async_computation | async-start | bytes 8192 | tf_op jit(solution)/shard_map/all_to_all | solution.py:284
  9.8 3.9 %convolution_convert_fusion.1.v_ref = bf16[1024,256]{1,0:T(8,128)(2,1)S(1)} fusion(bf16[1024,2048]{1,0:T(8,128)(2,1)} %bitcast.36, bf16[2048,256]{1,0:T(8,128)(2,1)} %param.10), kind=kOutput, calls=%fused_computation.4 | convolution fusion | flops 1074003968 | bytes 5767168 | tf_op jit(solution)/shard_map/dot_general | solution.py:278
  13.7 0.1 copy-done.6
  13.8 1.2 %convolution_convert_fusion.2.k_ref = bf16[1024,256]{1,0:T(8,128)(2,1)S(1)} fusion(bf16[1024,2048]{1,0:T(8,128)(2,1)S(1)} %bitcast.38, bf16[2048,256]{1,0:T(8,128)(2,1)S(1)} %copy-done.6), kind=kOutput, calls=%fused_computation.5 | convolution fusion | flops 1074003968 | bytes 5767168 | tf_op jit(solution)/shard_map/dot_general | solution.py:278
  15.1 1.1 %all-to-all-done = s32[8,1,3]{2,1,0:T(1,128)S(1)} async-done(((s32[8,1,3]{2,1,0:T(1,128)}), s32[8,1,3]{2,1,0:T(1,128)S(1)}, u32[]{:S(2)}, u32[]{:S(2)}) %all-to-all-start) | async-done | bytes 128 | tf_op jit(solution)/shard_map/all_to_all | solution.py:284
  16.4 1.5 %gather_fusion = bf16[24,64,256]{2,1,0:T(8,128)(2,1)} fusion(bf16[16,64,256]{2,1,0:T(8,128)(2,1)S(1)} %bitcast.29, s32[1024]{0:T(1024)S(1)} %pad_clamp_fusion), kind=kCustom, calls=%fused_computation | custom fusion | bytes 1572960 | tf_op jit(solution)/shard_map/gather | solution.py:288
  17.9 1.5 %gather_fusion.1 = bf16[24,64,256]{2,1,0:T(8,128)(2,1)} fusion(bf16[16,64,256]{2,1,0:T(8,128)(2,1)S(1)} %bitcast.28, s32[1024]{0:T(1024)S(1)} %pad_clamp_fusion), kind=kCustom, calls=%fused_computation.1 | custom fusion | bytes 1572960 | tf_op jit(solution)/shard_map/gather | solution.py:288
  19.4 2.7 %pad_maximum_fusion = bf16[8,3,64,512]{3,2,1,0:T(8,128)(2,1)} fusion(bf16[8,3,64,256]{3,2,1,0:T(8,128)(2,1)} %bitcast.31, bf16[8,3,64,256]{3,2,1,0:T(8,128)(2,1)} %bitcast.30), kind=kLoop, calls=%fused_computation.2 | loop fusion | flops 3145728 | bytes 3145728 | tf_op jit(solution)/shard_map/concatenate | solution.py:286
  22.1 4.9 %all-to-all-start.1 = ((bf16[8,3,64,512]{3,2,1,0:T(8,128)(2,1)}), bf16[8,3,64,512]{3,2,1,0:T(8,128)(2,1)}, u32[]{:S(2)}, u32[]{:S(2)}) async-start(bf16[8,3,64,512]{3,2,1,0:T(8,128)(2,1)} %pad_maximum_fusion), calls=%async_computation.1 | async-start | bytes 3145728 | tf_op jit(solution)/shard_map/all_to_all | solution.py:293
  27.2 0.1 copy.37
  27.3 0.1 reshape.100
  27.4 0.2 copy.36
  27.6 0.1 convert_reduce_fusion
  27.8 0.1 stack_reshape.3
  28.0 0.2 copy.39
  28.2 0.1 select_n.41
  28.3 0.1 broadcast_in_dim.92
  28.4 0.1 reshape.101.rem_bias_ref
  28.5 0.2 convert_reduce_fusion.2
  28.9 5.5 %convolution_convert_fusion.q_ref = bf16[1024,512]{1,0:T(8,128)(2,1)} fusion(bf16[1024,2048]{1,0:T(8,128)(2,1)} %bitcast.37, bf16[2048,512]{1,0:T(8,128)(2,1)S(1)} %copy-done), kind=kOutput, calls=%fused_computation.3 | convolution fusion | flops 2148007936 | bytes 7340032 | tf_op jit(solution)/shard_map/dot_general | solution.py:278
  34.4 29.2 %all-to-all-done.1 = bf16[8,3,64,512]{3,2,1,0:T(8,128)(2,1)} async-done(((bf16[8,3,64,512]{3,2,1,0:T(8,128)(2,1)}), bf16[8,3,64,512]{3,2,1,0:T(8,128)(2,1)}, u32[]{:S(2)}, u32[]{:S(2)}) %all-to-all-start.1) | async-done | bytes 1572896 | tf_op jit(solution)/shard_map/all_to_all | solution.py:293
  63.6 1.4 %copy-done.2 = bf16[1024,512]{1,0:T(8,128)(2,1)S(1)} copy-done((bf16[1024,512]{1,0:T(8,128)(2,1)S(1)}, bf16[1024,512]{1,0:T(8,128)(2,1)}, u32[]{:S(2)}) %copy-start.2) | copy-done | bytes 1048600
  65.0 6.4 %shard_map.73.att_ref = bf16[1024,512]{1,0:T(8,128)(2,1)S(1)} custom-call(s32[4]{0:T(128)S(1)} %copy-done.3, bf16[1024,512]{1,0:T(8,128)(2,1)S(1)} %copy-done.2, bf16[1024,256]{1,0:T(8,128)(2,1)S(1)} %convolution_convert_fusion.2.k_ref, bf16[1024,256]{1,0:T(8,128)(2,1)S(1)} %convolution_convert_fusion.1.v_ref, bf16[1536,512]{1,0:T(8,128)(2,1)} %bitcast.9.rem_ref, ...), custom_call_target="tpu_custom_call" | custom-call | tf_op jit(solution)/shard_map/pallas_call | solution.py:144
  71.4 27.6 %shard_map.74 = bf16[1024,512]{1,0:T(8,128)(2,1)S(1)} custom-call(bf16[1024,512]{1,0:T(8,128)(2,1)S(1)} %shard_map.73.att_ref, bf16[512,2048]{1,0:T(8,128)(2,1)S(1)} %copy-done.1), custom_call_target="tpu_custom_call" | custom-call | tf_op jit(solution)/shard_map/pallas_call | solution.py:248
  99.0 1.0 copy.42
  (32 shorter events, 0.8 us)
Async XLA Ops:
  0.0 28.9 %copy-start = (bf16[2048,512]{1,0:T(8,128)(2,1)S(1)}, bf16[2048,512]{1,0:T(8,128)(2,1)}, u32[]{:S(2)}) copy-start(bf16[2048,512]{1,0:T(8,128)(2,1)} %param.8) | copy-start | bytes 6291460
  2.5 13.7 %all-to-all-start = ((s32[8,1,3]{2,1,0:T(1,128)}), s32[8,1,3]{2,1,0:T(1,128)S(1)}, u32[]{:S(2)}, u32[]{:S(2)}) async-start(s32[8,1,3]{2,1,0:T(1,128)} %copy.33), calls=%async_computation | async-start | bytes 8192 | tf_op jit(solution)/shard_map/all_to_all | solution.py:284
  9.7 3.9 %copy-start.5 = (bf16[4,256,2048]{2,1,0:T(8,128)(2,1)S(1)}, bf16[4,256,2048]{2,1,0:T(8,128)(2,1)}, u32[]{:S(2)}) copy-start(bf16[4,256,2048]{2,1,0:T(8,128)(2,1)} %param.7) | copy-start | bytes 12582916
  9.8 4.1 %copy-start.6 = (bf16[2048,256]{1,0:T(8,128)(2,1)S(1)}, bf16[2048,256]{1,0:T(8,128)(2,1)}, u32[]{:S(2)}) copy-start(bf16[2048,256]{1,0:T(8,128)(2,1)} %param.9) | copy-start | bytes 3145732
  19.4 9.1 %copy-start.4 = (s32[4,4,32]{2,1,0:T(4,128)S(1)}, s32[4,4,32]{2,1,0:T(4,128)}, u32[]{:S(2)}) copy-start(s32[4,4,32]{2,1,0:T(4,128)} %param.12) | copy-start | bytes 6148
  22.1 41.4 %all-to-all-start.1 = ((bf16[8,3,64,512]{3,2,1,0:T(8,128)(2,1)}), bf16[8,3,64,512]{3,2,1,0:T(8,128)(2,1)}, u32[]{:S(2)}, u32[]{:S(2)}) async-start(bf16[8,3,64,512]{3,2,1,0:T(8,128)(2,1)} %pad_maximum_fusion), calls=%async_computation.1 | async-start | bytes 3145728 | tf_op jit(solution)/shard_map/all_to_all | solution.py:293
  28.9 34.7 %copy-start.3 = (s32[4]{0:T(128)S(1)}, s32[4]{0:T(128)}, u32[]{:S(2)}) copy-start(s32[4]{0:T(128)} %length_ref.1) | copy-start | bytes 52
  63.6 7.8 %copy-start.1 = (bf16[512,2048]{1,0:T(8,128)(2,1)S(1)}, bf16[512,2048]{1,0:T(8,128)(2,1)}, u32[]{:S(2)}) copy-start(bf16[512,2048]{1,0:T(8,128)(2,1)} %weight_ref.1) | copy-start | bytes 6291460
  63.6 1.4 %copy-start.2 = (bf16[1024,512]{1,0:T(8,128)(2,1)S(1)}, bf16[1024,512]{1,0:T(8,128)(2,1)}, u32[]{:S(2)}) copy-start(bf16[1024,512]{1,0:T(8,128)(2,1)} %convolution_convert_fusion.q_ref) | copy-start | bytes 3145732
where the time goes:
time: 100 us
  Pallas kernels  34 us (34%)
  waiting for transfers between devices  30.3 us (30%)
  starting transfers between devices  12.2 us (12%)
  matrix products  10.6 us (11%)
  local copies, waits for them, and re-layouts  7.94 us (8%)
  other arithmetic  4.71 us (5%)
    all_to_all x1, waiting for transfers between devices, shards(): got = lax.all_to_all(picked, 'kv', split_axis=0, concat_axis=0, tiled=True)  29.2 us
    pallas_call x1, Pallas kernels, mix(): pl.pallas_call(functools.partial(mix_kernel, steps, tp), out_shape=jax.Sh...  27.6 us
    dot_general x3, matrix products, project(): jnp.dot(flat_rows, weight, preferred_element_type=jnp.float32)  10.6 us
    all_to_all x1, starting transfers between devices, shards(): lax.all_to_all(requests, 'kv', split_axis=0, concat_axis=0, tiled=True)  7.29 us
    pallas_call x1, Pallas kernels, attend(): pl.pallas_call(functools.partial(attend_kernel, positions, kv_local, per_...  6.41 us
    all_to_all x1, starting transfers between devices, shards(): got = lax.all_to_all(picked, 'kv', split_axis=0, concat_axis=0, tiled=True)  4.9 us
    gather x2, local copies, waits for them, and re-layouts, shards(): table.reshape(owned, KB, kv_local * HD)[asked]  3.02 us
    concatenate x1, other arithmetic, shards(): jnp.concatenate([table.reshape(owned, KB, kv_local * HD)[asked] for table...  2.68 us
  transfers between devices with their start and end apart: 2, of which 2 were waited for; matrix products, arithmetic and copies ran while one was open for 12% of the time, Pallas kernels for 0%

commit v1 on v0

v1 whole, which is shorter than its diff:
```python
import functools

import jax
import jax.numpy as jnp
from jax import lax
from jax.experimental import pallas as pl
from jax.experimental.pallas import tpu as pltpu
from jax.sharding import PartitionSpec as P

HD = 128
KB = 64
MASKED = -1e30
PIECES = 2
STEP_ROWS = 128
MESH = pl.DeviceIdType.MESH


def spans(batch_size, devices, positions):
    seq = devices * positions
    total = seq + seq // 2
    longest = [min(seq, (total - (batch_size - 1 - j)) // (j + 1)) for j in range(batch_size)]
    return tuple(-(-length // positions) for length in longest)


def layer_kernel(
    reach, columns, kv_local, per_group, tp,
    length_ref, x_hbm, wq_hbm, wk_hbm, wv_hbm, wo_hbm, chosen_ref, out_ref,
    x_ref, wq_ref, wkv_ref, wo_ref, stage_ref, kv_ref, q_ref,
    top_ref, total_ref, acc_ref, att_ref,
    pair_out, pair_in, far_out, far_in, near, mixed_ref,
    load_sem, z_sent, x_sent, got, pair_sent, pair_got, far_sent, far_got,
):
    batch_size, positions, _ = x_ref.shape
    slots, devices = kv_ref.shape[:2]
    rows_z = devices // columns
    per_dev = positions // KB
    half = kv_local * HD
    rows = per_group * positions
    width = out_ref.shape[-1]
    piece_rows = positions // PIECES
    mix_steps = positions // STEP_ROWS
    scaling = HD ** (-0.5)
    contract = (((1,), (1,)), ((), ()))

    device = lax.axis_index("kv")
    z = device // columns
    x = lax.rem(device, columns)
    me = lax.axis_index("tp")
    core = lax.rem(me, 2)
    chip = me // 2
    chips = tp // 2
    partner = me + 1 - 2 * core

    def live_at(r):
        return sum([(r < reach[j]).astype(jnp.int32) for j in range(slots)])

    def column(i):
        return lax.rem(x + i, columns)

    def twin(off):
        return lax.rem(chip + off, chips) * 2 + core

    mine = live_at(device)
    row_live = live_at(z * columns)
    next_live = live_at((z + 1) * columns)

    loads = [
        pltpu.make_async_copy(wk_hbm, wkv_ref.at[:, pl.ds(0, half)], load_sem.at[0]),
        pltpu.make_async_copy(wv_hbm, wkv_ref.at[:, pl.ds(half, half)], load_sem.at[1]),
        pltpu.make_async_copy(wq_hbm, wq_ref, load_sem.at[2]),
        pltpu.make_async_copy(wo_hbm, wo_ref, load_sem.at[3]),
    ]

    def x_load(b):
        return pltpu.make_async_copy(x_hbm.at[b], x_ref.at[b], load_sem.at[4 + b])

    loads[0].start()
    loads[1].start()
    for b in range(batch_size):
        x_load(b).start()
    loads[2].start()
    loads[3].start()

    barrier = pltpu.get_barrier_semaphore()

    def greet(**where):
        pl.semaphore_signal(barrier, inc=1, device_id=where, device_id_type=MESH)

    greet(tp=partner)
    for off in range(1, chips):
        greet(tp=twin(off))
    for i in range(1, columns):
        greet(kv=z * columns + column(i))

    @pl.when(z > 0)
    def _():
        greet(kv=device - columns)

    @pl.when(z < rows_z - 1)
    def _():
        greet(kv=device + columns)

    lengths = [length_ref[b] for b in range(batch_size)]
    ranks = []
    for b in range(batch_size):
        ahead = [
            (lengths[o] >= lengths[b] if o < b else lengths[o] > lengths[b]).astype(jnp.int32)
            for o in range(batch_size) if o != b
        ]
        ranks.append(sum(ahead))

    def holder(j):
        return sum([jnp.where(ranks[b] == j, b, 0) for b in range(batch_size)])

    loads[0].wait()
    loads[1].wait()

    def project_kv(b, carry):
        x_load(b).wait()
        stage_ref[b] = jnp.dot(
            x_ref[b], wkv_ref[...], preferred_element_type=jnp.float32
        ).astype(jnp.bfloat16)
        return carry

    lax.fori_loop(0, batch_size, project_kv, 0)
    pl.semaphore_wait(
        barrier,
        chips + columns - 1
        + (z > 0).astype(jnp.int32) + (z < rows_z - 1).astype(jnp.int32),
    )

    def piece(j, c, p):
        return kv_ref.at[j, c, pl.ds(p * piece_rows, piece_rows)]

    def z_copy(j, c, p):
        return pltpu.make_async_remote_copy(
            src_ref=piece(j, c, p), dst_ref=piece(j, c, p),
            send_sem=z_sent.at[j, c // columns, p], recv_sem=got.at[j, c, p],
            device_id={"kv": device + columns}, device_id_type=MESH,
        )

    def x_copy(j, c, p, i):
        return pltpu.make_async_remote_copy(
            src_ref=piece(j, c, p), dst_ref=piece(j, c, p),
            send_sem=x_sent.at[j, c // columns, i - 1, p], recv_sem=got.at[j, c, p],
            device_id={"kv": z * columns + column(i)}, device_id_type=MESH,
        )

    def arrival(j, c, p):
        return pltpu.make_async_remote_copy(
            src_ref=piece(j, c, p), dst_ref=piece(j, c, p),
            send_sem=z_sent.at[j, c // columns, p], recv_sem=got.at[j, c, p],
            device_id={"tp": partner}, device_id_type=MESH,
        )

    def each_send(j, c, p, act):
        own = c == device

        @pl.when(j < next_live)
        def _():
            act(z_copy(j, c, p))

        for i in range(1, columns):
            wanted = (j < live_at(z * columns + column(i))) & (
                jnp.logical_not(own) | (column(i) > x)
            )

            @pl.when(wanted)
            def _():
                act(x_copy(j, c, p, i))

    def send_own(j):
        kv_ref[j, device] = stage_ref[holder(j)]
        for p in range(PIECES):
            each_send(j, device, p, lambda copy: copy.start())

    send_own(0)

    loads[2].wait()

    def project_q(b, carry):
        queries = jnp.dot(
            x_ref[b], wq_ref[...], preferred_element_type=jnp.float32
        ).astype(jnp.bfloat16)
        for n in range(kv_local * per_group):
            q_ref[b, n // per_group, pl.ds(lax.rem(n, per_group) * positions, positions), :] = (
                queries[:, n * HD:(n + 1) * HD]
            )
        return carry

    lax.fori_loop(0, batch_size, project_q, 0)
    loads[3].wait()

    def named(names, c):
        segment = lax.broadcasted_iota(jnp.int32, (per_dev, positions), 1) // KB
        bias = jnp.full((per_dev, positions), MASKED, jnp.float32)
        for i in range(per_dev):
            hit = jnp.max(
                jnp.where(names == c * per_dev + i, 0.0, MASKED), axis=1, keepdims=True
            )
            bias = jnp.where(segment == i, hit, bias)
        return jnp.broadcast_to(bias[:, None, :], (per_dev, KB, positions)).reshape(
            positions, positions
        )

    def scores(b, j, c, h, bias):
        raw = lax.dot_general(
            q_ref[b, h], kv_ref[j, c, :, h * HD:(h + 1) * HD], contract,
            preferred_element_type=jnp.float32,
        )
        shaped = (raw * scaling).reshape(per_group, positions, positions) + bias[None]
        return shaped.reshape(rows, positions)

    def weigh(j, c, h, raised):
        return jnp.dot(
            raised.astype(jnp.bfloat16), kv_ref[j, c, :, half + h * HD:half + (h + 1) * HD],
            preferred_element_type=jnp.float32,
        )

    def wide(value):
        return jnp.concatenate([value] * (positions // HD), axis=1)

    def attend_own(j):
        b = holder(j)
        names = chosen_ref[b]
        before = named(names, device)
        home = device * per_dev + lax.broadcasted_iota(jnp.int32, names.shape, 0)
        copies = jnp.sum(jnp.where(names == home, 1.0, 0.0), axis=1, keepdims=True)
        same = jnp.log(jnp.maximum(copies, 1.0))
        same = jnp.broadcast_to(same[:, None, :], (per_dev, KB, positions)).reshape(
            positions, positions
        )
        at_row = lax.broadcasted_iota(jnp.int32, (positions, positions), 0)
        at_col = lax.broadcasted_iota(jnp.int32, (positions, positions), 1)
        bias = jnp.where(at_col < at_row, before, jnp.where(at_col == at_row, same, MASKED))
        for h in range(kv_local):
            s = scores(b, j, device, h, bias)
            top = jnp.broadcast_to(jnp.max(s, axis=1, keepdims=True), (rows, HD))
            raised = jnp.exp(s - wide(top))
            top_ref[h] = top
            total_ref[h] = jnp.broadcast_to(jnp.sum(raised, axis=1, keepdims=True), (rows, HD))
            acc_ref[h] = weigh(j, device, h, raised)

    def attend_far(j, c):
        b = holder(j)
        bias = named(chosen_ref[b], c)
        for h in range(kv_local):
            s = scores(b, j, c, h, bias)
            old = top_ref[h]
            top = jnp.maximum(old, jnp.max(s, axis=1, keepdims=True))
            fade = jnp.exp(old - top)
            raised = jnp.exp(s - wide(top))
            top_ref[h] = top
            total_ref[h] = total_ref[h] * fade + jnp.sum(raised, axis=1, keepdims=True)
            acc_ref[h] = acc_ref[h] * fade + weigh(j, c, h, raised)

    def attend_end(j):
        live = sum(
            [jnp.where(ranks[b] == j, lengths[b], 0) for b in range(batch_size)]
        ) - device * positions
        living = lax.broadcasted_iota(jnp.int32, (positions, HD), 0) < live
        for h in range(kv_local):
            done = acc_ref[h] / total_ref[h]
            for g in range(per_group):
                n = h * per_group + g
                att_ref[j, :, n * HD:(n + 1) * HD] = jnp.where(
                    living, done[g * positions:(g + 1) * positions], 0.0
                ).astype(jnp.bfloat16)

    def group_sum(j, m, off, side):
        start = (lax.rem(chip + off, chips) * 2 + side) * width
        return jnp.dot(
            att_ref[j, m * STEP_ROWS:(m + 1) * STEP_ROWS, :],
            wo_ref[:, pl.ds(pl.multiple_of(start, width), width)],
            preferred_element_type=jnp.float32,
        ).astype(jnp.bfloat16)

    def pair_copy(i):
        return pltpu.make_async_remote_copy(
            src_ref=pair_out.at[i], dst_ref=pair_in.at[i],
            send_sem=pair_sent.at[i], recv_sem=pair_got.at[i],
            device_id={"tp": partner}, device_id_type=MESH,
        )

    def far_copy(i, off):
        return pltpu.make_async_remote_copy(
            src_ref=far_out.at[off - 1, i], dst_ref=far_in.at[off - 1, i],
            send_sem=far_sent.at[off - 1, i], recv_sem=far_got.at[off - 1, i],
            device_id={"tp": twin(off)}, device_id_type=MESH,
        )

    def mix(j):
        for m in range(mix_steps):
            i = j * mix_steps + m
            for off in range(chips):
                pair_out[i, off] = group_sum(j, m, off, 1 - core)
            pair_copy(i).start()
        for m in range(mix_steps):
            i = j * mix_steps + m
            sums = [group_sum(j, m, off, core).astype(jnp.float32) for off in range(chips)]
            pair_copy(i).wait_recv()
            for off in range(1, chips):
                both = sums[off] + pair_in[i, off].astype(jnp.float32)
                far_out[off - 1, i] = both.astype(jnp.bfloat16)
                far_copy(i, off).start()
            near[i] = sums[0] + pair_in[i, 0].astype(jnp.float32)

    def slot(j, carry):
        used = j < mine

        @pl.when(used)
        def _():
            attend_own(j)

        def step(t, carry):
            d = t // columns
            i = lax.rem(t, columns)
            c = (z - d) * columns + column(i)
            relayed = (i == 0) & (d > 0)
            taken = used & (i > 0) & ((d > 0) | (column(i) < x))

            @pl.when(relayed)
            def _():
                for p in range(PIECES):
                    arrival(j, c, p).wait_recv()
                    each_send(j, c, p, lambda copy: copy.start())

            @pl.when(taken)
            def _():
                for p in range(PIECES):
                    arrival(j, c, p).wait_recv()

            @pl.when((relayed & used) | taken)
            def _():
                attend_far(j, c)

            return carry

        lax.fori_loop(0, (z + 1) * columns, step, 0)

        @pl.when(j + 1 < row_live)
        def _():
            send_own(j + 1)

        @pl.when(used)
        def _():
            attend_end(j)
            mix(j)

        return carry

    lax.fori_loop(0, row_live, slot, 0)

    def finish(j, carry):
        for m in range(mix_steps):
            i = j * mix_steps + m
            pair_copy(i).wait_send()
            mixed = near[i]
            for off in range(1, chips):
                far_copy(i, off).wait()
                mixed = mixed + far_in[off - 1, i].astype(jnp.float32)
            mixed_ref[j, m * STEP_ROWS:(m + 1) * STEP_ROWS, :] = mixed.astype(jnp.bfloat16)
        return carry

    lax.fori_loop(0, mine, finish, 0)

    def blank(j, carry):
        mixed_ref[j] = jnp.zeros(mixed_ref.shape[1:], jnp.bfloat16)
        return carry

    lax.fori_loop(mine, slots, blank, 0)
    for b in range(batch_size):
        out_ref[b] = mixed_ref[ranks[b]]

    def drain(j, carry):
        def back(d, carry):
            c = (z - d) * columns + x
            for p in range(PIECES):
                each_send(j, c, p, lambda copy: copy.wait_send())
            return carry

        return lax.fori_loop(0, z + 1, back, carry)

    lax.fori_loop(0, row_live, drain, 0)


def columns_of(devices):
    return 1 << ((devices.bit_length() - 1) // 2)


def shards(inputs, query_weight, key_weight, value_weight, out_weight, chosen, lengths):
    batch_size, positions, model_width = inputs.shape
    kv_local = key_weight.shape[1] // HD
    heads_local = query_weight.shape[1] // HD
    per_group = heads_local // kv_local
    devices = lax.axis_size("kv")
    tp = lax.axis_size("tp")
    chips = tp // 2
    columns = columns_of(devices)
    reach = spans(batch_size, devices, positions)
    width = out_weight.shape[1] // tp
    steps = batch_size * (positions // STEP_ROWS)
    rows = per_group * positions
    bf16, f32 = jnp.bfloat16, jnp.float32
    vmem = pl.BlockSpec(memory_space=pltpu.VMEM)
    hbm = pl.BlockSpec(memory_space=pl.ANY)
    dma = pltpu.SemaphoreType.DMA
    pair = pltpu.VMEM((steps, chips, STEP_ROWS, width), bf16)
    far = pltpu.VMEM((chips - 1, steps, STEP_ROWS, width), bf16)
    return pl.pallas_call(
        functools.partial(layer_kernel, reach, columns, kv_local, per_group, tp),
        out_shape=jax.ShapeDtypeStruct((batch_size, positions, width), bf16),
        in_specs=[pl.BlockSpec(memory_space=pltpu.SMEM)] + [hbm] * 5 + [vmem],
        out_specs=vmem,
        scratch_shapes=[
            pltpu.VMEM(inputs.shape, bf16),
            pltpu.VMEM(query_weight.shape, bf16),
            pltpu.VMEM((model_width, 2 * kv_local * HD), bf16),
            pltpu.VMEM(out_weight.shape, bf16),
            pltpu.VMEM((batch_size, positions, 2 * kv_local * HD), bf16),
            pltpu.VMEM((batch_size, devices, positions, 2 * kv_local * HD), bf16),
            pltpu.VMEM((batch_size, kv_local, rows, HD), bf16),
            pltpu.VMEM((kv_local, rows, HD), f32),
            pltpu.VMEM((kv_local, rows, HD), f32),
            pltpu.VMEM((kv_local, rows, HD), f32),
            pltpu.VMEM((batch_size, positions, heads_local * HD), bf16),
            pair, pair, far, far,
            pltpu.VMEM((steps, STEP_ROWS, width), f32),
            pltpu.VMEM((batch_size, positions, width), bf16),
            dma((4 + batch_size,)),
            dma((batch_size, devices // columns, PIECES)),
            dma((batch_size, devices // columns, max(columns - 1, 1), PIECES)),
            dma((batch_size, devices, PIECES)),
            dma((steps,)), dma((steps,)),
            dma((chips - 1, steps)), dma((chips - 1, steps)),
        ],
        compiler_params=pltpu.CompilerParams(
            collective_id=0, has_side_effects=True, vmem_limit_bytes=60 * 2**20
        ),
    )(lengths, inputs, query_weight, key_weight, value_weight, out_weight, chosen)


def solution(mesh):
    placed = (
        P(None, "kv", None),
        P(None, "tp"),
        P(None, "tp"),
        P(None, "tp"),
        P("tp", None),
        P(None, "kv", None),
        P(),
    )
    return jax.shard_map(
        shards, mesh=mesh, in_specs=placed, out_specs=P(None, "kv", "tp"), check_vma=False
    )
```

time: 100 us -> 70.5 us (0.70)
  the two profiles are of different devices: /device:TPU:0 before, /device:TPU:8 now
where the time goes in v1:
time: 70.5 us; the launch traced here: 70.3 us
  Pallas kernels  68 us (96%)
  local copies, waits for them, and re-layouts  2.26 us (3%)
    pallas_call x1, Pallas kernels, shards(): pl.pallas_call(functools.partial(layer_kernel, reach, columns, kv_local,...  68 us
    unnamed x1, local copies, waits for them, and re-layouts  2.26 us

profile of v1, /device:TPU:8, one launch (start us, length us, event | category | flops | bytes accessed | tf_op | source)
XLA Modules:
  0.0 70.3 jit_solution(10244224820212522861)
XLA Ops:
  0.0 68.0 %shard_map.73 = bf16[4,256,512]{2,1,0:T(8,128)(2,1)} custom-call(s32[4]{0:T(128)} %length_ref.1, bf16[4,256,2048]{2,1,0:T(8,128)(2,1)} %x_hbm.1, bf16[2048,512]{1,0:T(8,128)(2,1)} %wq_hbm.1, bf16[2048,256]{1,0:T(8,128)(2,1)} %wk_hbm.1, bf16[2048,256]{1,0:T(8,128)(2,1)} %wv_hbm.1, bf16[512,2048]{1,0:T(8,128)(2,1)} %wo_hbm.1, s32[4,4,32]{2,1,0:T(4,128)} %chosen_ref.1), custom_call_target="tpu_custom_call" | custom-call | tf_op jit(solution)/shard_map/pallas_call | solution.py:410
  68.0 2.3 %copy.9 = bf16[4,256,512]{2,1,0:T(8,128)(2,1)} copy(bf16[4,256,512]{2,1,0:T(8,128)(2,1)} %shard_map.73) | data formatting | bytes 2097152

commit v2 on v1

--- a/solution.py
+++ b/solution.py
@@ -19,13 +19,17 @@
     seq = devices * positions
     total = seq + seq // 2
     longest = [min(seq, (total - (batch_size - 1 - j)) // (j + 1)) for j in range(batch_size)]
-    return tuple(-(-length // positions) for length in longest)
+    whole = tuple(-(-length // positions) for length in longest)
+    short = tuple(
+        min(full, -(-devices * 3 // (8 * j)) if j else devices) for j, full in enumerate(whole)
+    )
+    return short, whole
 
 
 def layer_kernel(
     reach, columns, kv_local, per_group, tp,
     length_ref, x_hbm, wq_hbm, wk_hbm, wv_hbm, wo_hbm, chosen_ref, out_ref,
-    x_ref, wq_ref, wkv_ref, wo_ref, stage_ref, kv_ref, q_ref,
+    x_ref, wq_ref, wkv_ref, wo_ref, kv_ref, q_ref,
     top_ref, total_ref, acc_ref, att_ref,
     pair_out, pair_in, far_out, far_in, near, mixed_ref,
     load_sem, z_sent, x_sent, got, pair_sent, pair_got, far_sent, far_got,
@@ -112,17 +116,6 @@
     def holder(j):
         return sum([jnp.where(ranks[b] == j, b, 0) for b in range(batch_size)])
 
-    loads[0].wait()
-    loads[1].wait()
-
-    def project_kv(b, carry):
-        x_load(b).wait()
-        stage_ref[b] = jnp.dot(
-            x_ref[b], wkv_ref[...], preferred_element_type=jnp.float32
-        ).astype(jnp.bfloat16)
-        return carry
-
-    lax.fori_loop(0, batch_size, project_kv, 0)
     pl.semaphore_wait(
         barrier,
         chips + columns - 1
@@ -170,26 +163,36 @@
                 act(x_copy(j, c, p, i))
 
     def send_own(j):
-        kv_ref[j, device] = stage_ref[holder(j)]
         for p in range(PIECES):
             each_send(j, device, p, lambda copy: copy.start())
 
-    send_own(0)
-
+    loads[0].wait()
+    loads[1].wait()
+    for b in range(batch_size):
+        x_load(b).wait()
+
+    def project_kv(j, carry):
+        kv_ref[j, device] = jnp.dot(
+            x_ref[holder(j)], wkv_ref[...], preferred_element_type=jnp.float32
+        ).astype(jnp.bfloat16)
+
+        @pl.when((j == 0) | (z == 0))
+        def _():
+            send_own(j)
+
+        return carry
+
+    lax.fori_loop(0, row_live, project_kv, 0)
     loads[2].wait()
-
-    def project_q(b, carry):
+    loads[3].wait()
+
+    def project_q(j):
         queries = jnp.dot(
-            x_ref[b], wq_ref[...], preferred_element_type=jnp.float32
+            x_ref[holder(j)], wq_ref[...], preferred_element_type=jnp.float32
         ).astype(jnp.bfloat16)
         for n in range(kv_local * per_group):
-            q_ref[b, n // per_group, pl.ds(lax.rem(n, per_group) * positions, positions), :] = (
-                queries[:, n * HD:(n + 1) * HD]
-            )
-        return carry
-
-    lax.fori_loop(0, batch_size, project_q, 0)
-    loads[3].wait()
+            h, g = n // per_group, n % per_group
+            q_ref[h, g * positions:(g + 1) * positions, :] = queries[:, n * HD:(n + 1) * HD]
 
     def named(names, c):
         segment = lax.broadcasted_iota(jnp.int32, (per_dev, positions), 1) // KB
@@ -203,9 +206,9 @@
             positions, positions
         )
 
-    def scores(b, j, c, h, bias):
+    def scores(j, c, h, bias):
         raw = lax.dot_general(
-            q_ref[b, h], kv_ref[j, c, :, h * HD:(h + 1) * HD], contract,
+            q_ref[h], kv_ref[j, c, :, h * HD:(h + 1) * HD], contract,
             preferred_element_type=jnp.float32,
         )
         shaped = (raw * scaling).reshape(per_group, positions, positions) + bias[None]
@@ -221,8 +224,7 @@
         return jnp.concatenate([value] * (positions // HD), axis=1)
 
     def attend_own(j):
-        b = holder(j)
-        names = chosen_ref[b]
+        names = chosen_ref[holder(j)]
         before = named(names, device)
         home = device * per_dev + lax.broadcasted_iota(jnp.int32, names.shape, 0)
         copies = jnp.sum(jnp.where(names == home, 1.0, 0.0), axis=1, keepdims=True)
@@ -234,7 +236,7 @@
         at_col = lax.broadcasted_iota(jnp.int32, (positions, positions), 1)
         bias = jnp.where(at_col < at_row, before, jnp.where(at_col == at_row, same, MASKED))
         for h in range(kv_local):
-            s = scores(b, j, device, h, bias)
+            s = scores(j, device, h, bias)
             top = jnp.broadcast_to(jnp.max(s, axis=1, keepdims=True), (rows, HD))
             raised = jnp.exp(s - wide(top))
             top_ref[h] = top
@@ -242,10 +244,9 @@
             acc_ref[h] = weigh(j, device, h, raised)
 
     def attend_far(j, c):
-        b = holder(j)
-        bias = named(chosen_ref[b], c)
+        bias = named(chosen_ref[holder(j)], c)
         for h in range(kv_local):
-            s = scores(b, j, c, h, bias)
+            s = scores(j, c, h, bias)
             old = top_ref[h]
             top = jnp.maximum(old, jnp.max(s, axis=1, keepdims=True))
             fade = jnp.exp(old - top)
@@ -305,42 +306,57 @@
                 far_copy(i, off).start()
             near[i] = sums[0] + pair_in[i, 0].astype(jnp.float32)
 
+    def relay(t):
+        j = t // z
+        d = lax.rem(t, z)
+        c = device - (d + 1) * columns
+
+        @pl.when((d == 0) & (j > 0))
+        def _():
+            send_own(j)
+
+        for p in range(PIECES):
+            arrival(j, c, p).wait_recv()
+            each_send(j, c, p, lambda copy: copy.start())
+
+    def take(j, c):
+        for p in range(PIECES):
+            arrival(j, c, p).wait_recv()
+        attend_far(j, c)
+
     def slot(j, carry):
         used = j < mine
 
         @pl.when(used)
         def _():
+            project_q(j)
             attend_own(j)
+
+        @pl.when((j == 0) & (z > 0))
+        def _():
+            relay(0)
 
         def step(t, carry):
             d = t // columns
             i = lax.rem(t, columns)
             c = (z - d) * columns + column(i)
-            relayed = (i == 0) & (d > 0)
-            taken = used & (i > 0) & ((d > 0) | (column(i) < x))
-
-            @pl.when(relayed)
+            ahead = j * z + d
+
+            @pl.when((i == 0) & (d > 0) & (ahead < row_live * z))
             def _():
-                for p in range(PIECES):
-                    arrival(j, c, p).wait_recv()
-                    each_send(j, c, p, lambda copy: copy.start())
-
-            @pl.when(taken)
-            def _():
-                for p in range(PIECES):
-                    arrival(j, c, p).wait_recv()
-
-            @pl.when((relayed & used) | taken)
+                relay(ahead)
+
+            @pl.when(used & (i == 0) & (d > 0))
             def _():
                 attend_far(j, c)
 
+            @pl.when(used & (i > 0) & ((d > 0) | (column(i) < x)))
+            def _():
+                take(j, c)
+
             return carry
 
         lax.fori_loop(0, (z + 1) * columns, step, 0)
-
-        @pl.when(j + 1 < row_live)
-        def _():
-            send_own(j + 1)
 
         @pl.when(used)
         def _():
@@ -388,7 +404,10 @@
     return 1 << ((devices.bit_length() - 1) // 2)
 
 
-def shards(inputs, query_weight, key_weight, value_weight, out_weight, chosen, lengths):
+def layer(
+    reach, collective_id,
+    inputs, query_weight, key_weight, value_weight, out_weight, chosen, lengths,
+):
     batch_size, positions, model_width = inputs.shape
     kv_local = key_weight.shape[1] // HD
     heads_local = query_weight.shape[1] // HD
@@ -397,7 +416,6 @@
     tp = lax.axis_size("tp")
     chips = tp // 2
     columns = columns_of(devices)
-    reach = spans(batch_size, devices, positions)
     width = out_weight.shape[1] // tp
     steps = batch_size * (positions // STEP_ROWS)
     rows = per_group * positions
@@ -417,9 +435,8 @@
             pltpu.VMEM(query_weight.shape, bf16),
             pltpu.VMEM((model_width, 2 * kv_local * HD), bf16),
             pltpu.VMEM(out_weight.shape, bf16),
-            pltpu.VMEM((batch_size, positions, 2 * kv_local * HD), bf16),
             pltpu.VMEM((batch_size, devices, positions, 2 * kv_local * HD), bf16),
-            pltpu.VMEM((batch_size, kv_local, rows, HD), bf16),
+            pltpu.VMEM((kv_local, rows, HD), bf16),
             pltpu.VMEM((kv_local, rows, HD), f32),
             pltpu.VMEM((kv_local, rows, HD), f32),
             pltpu.VMEM((kv_local, rows, HD), f32),
@@ -435,9 +452,22 @@
             dma((chips - 1, steps)), dma((chips - 1, steps)),
         ],
         compiler_params=pltpu.CompilerParams(
-            collective_id=0, has_side_effects=True, vmem_limit_bytes=60 * 2**20
+            collective_id=collective_id, has_side_effects=True, vmem_limit_bytes=60 * 2**20
         ),
     )(lengths, inputs, query_weight, key_weight, value_weight, out_weight, chosen)
+
+
+def shards(*args):
+    inputs, lengths = args[0], args[-1]
+    batch_size, positions, _ = inputs.shape
+    short, whole = spans(batch_size, lax.axis_size("kv"), positions)
+    longer = [jnp.sum(lengths > span * positions) <= j for j, span in enumerate(short)]
+    return lax.cond(
+        functools.reduce(jnp.logical_and, longer),
+        functools.partial(layer, short, 0),
+        functools.partial(layer, whole, 1),
+        *args,
+    )
 
 
 def solution(mesh):

time: 70.5 us -> 45.3 us (0.64)
  the two profiles are of different devices: /device:TPU:8 before, /device:TPU:25 now
where the time goes in v2:
time: 45.3 us; the launch traced here: 44.6 us
  Pallas kernels  39.7 us (88%)
  between operations  2.56 us (6%)
  other arithmetic  1.38 us (3%)
  local copies, waits for them, and re-layouts  0.97 us (2%)
    pallas_call x1, Pallas kernels, layer(): pl.pallas_call(functools.partial(layer_kernel, reach, columns, kv_local,...  39.7 us
    reduce_sum x1, other arithmetic, shards(): jnp.sum(lengths > span * positions) <= j  1.38 us
    unnamed x1, local copies, waits for them, and re-layouts  0.97 us

profile of v2, /device:TPU:25, one launch (start us, length us, event | category | flops | bytes accessed | tf_op | source)
XLA Modules:
  0.0 44.6 jit_solution(16997023026165730645)
XLA Ops:
  0.0 1.4 %fusion.3 = (s32[]{:T(128)}, s32[]{:T(128)}, s32[]{:T(128)}, s32[]{:T(128)}) fusion(s32[4]{0:T(128)} %param.15), kind=kLoop, calls=%fused_computation.7 | loop fusion | flops 44 | bytes 32 | tf_op jit(solution)/shard_map/reduce_sum | solution.py:464
  3.9 39.7 %conditional.1 = (bf16[4,256,512]{2,1,0:T(8,128)(2,1)S(1)}) conditional(s32[]{:T(128)} %convert_element_type.19, (s32[4]{0:T(128)}, bf16[4,256,2048]{2,1,0:T(8,128)(2,1)}, bf16[2048,512]{1,0:T(8,128)(2,1)}, bf16[2048,256]{1,0:T(8,128)(2,1)}, bf16[2048,256]{1,0:T(8,128)(2,1)}, /*index=5*/bf16[512,2048]{1,0:T(8,128)(2,1)}, ...), branch_computations={%region_4.0_spmd, %region_5.0_spmd} | conditional | bytes 8 | solution.py:465
  3.9 39.7 %branch_1_fun.1 = bf16[4,256,512]{2,1,0:T(8,128)(2,1)S(1)} custom-call(s32[4]{0:T(128)} %get-tuple-element.43.length_ref, bf16[4,256,2048]{2,1,0:T(8,128)(2,1)} %get-tuple-element.44.x_hbm, bf16[2048,512]{1,0:T(8,128)(2,1)} %get-tuple-element.45.wq_hbm, bf16[2048,256]{1,0:T(8,128)(2,1)} %get-tuple-element.46.wk_hbm, ...), custom_call_target="tpu_custom_call" | custom-call | tf_op jit(solution)/shard_map/cond/branch_1_fun/pallas_call | solution.py:428
  43.6 1.0 %copy.13 = bf16[4,256,512]{2,1,0:T(8,128)(2,1)} copy(bf16[4,256,512]{2,1,0:T(8,128)(2,1)S(1)} %get-tuple-element.50) | data formatting | bytes 2097152

commit v3 on v2

--- a/solution.py
+++ b/solution.py
@@ -28,8 +28,8 @@
 
 def layer_kernel(
     reach, columns, kv_local, per_group, tp,
-    length_ref, x_hbm, wq_hbm, wk_hbm, wv_hbm, wo_hbm, chosen_ref, out_ref,
-    x_ref, wq_ref, wkv_ref, wo_ref, kv_ref, q_ref,
+    length_hbm, x_hbm, wq_hbm, wk_hbm, wv_hbm, wo_hbm, chosen_hbm, out_ref,
+    length_ref, chosen_ref, x_ref, wq_ref, wkv_ref, wo_ref, kv_ref, q_ref,
     top_ref, total_ref, acc_ref, att_ref,
     pair_out, pair_in, far_out, far_in, near, mixed_ref,
     load_sem, z_sent, x_sent, got, pair_sent, pair_got, far_sent, far_got,
@@ -73,17 +73,19 @@
         pltpu.make_async_copy(wv_hbm, wkv_ref.at[:, pl.ds(half, half)], load_sem.at[1]),
         pltpu.make_async_copy(wq_hbm, wq_ref, load_sem.at[2]),
         pltpu.make_async_copy(wo_hbm, wo_ref, load_sem.at[3]),
+        pltpu.make_async_copy(length_hbm, length_ref, load_sem.at[4]),
+        pltpu.make_async_copy(chosen_hbm, chosen_ref, load_sem.at[5]),
     ]
 
     def x_load(b):
-        return pltpu.make_async_copy(x_hbm.at[b], x_ref.at[b], load_sem.at[4 + b])
-
+        return pltpu.make_async_copy(x_hbm.at[b], x_ref.at[b], load_sem.at[6 + b])
+
+    loads[4].start()
+    for b in range(batch_size):
+        x_load(b).start()
     loads[0].start()
     loads[1].start()
-    for b in range(batch_size):
-        x_load(b).start()
-    loads[2].start()
-    loads[3].start()
+    loads[5].start()
 
     barrier = pltpu.get_barrier_semaphore()
 
@@ -104,6 +106,7 @@
     def _():
         greet(kv=device + columns)
 
+    loads[4].wait()
     lengths = [length_ref[b] for b in range(batch_size)]
     ranks = []
     for b in range(batch_size):
@@ -116,12 +119,6 @@
     def holder(j):
         return sum([jnp.where(ranks[b] == j, b, 0) for b in range(batch_size)])
 
-    pl.semaphore_wait(
-        barrier,
-        chips + columns - 1
-        + (z > 0).astype(jnp.int32) + (z < rows_z - 1).astype(jnp.int32),
-    )
-
     def piece(j, c, p):
         return kv_ref.at[j, c, pl.ds(p * piece_rows, piece_rows)]
 
@@ -171,20 +168,31 @@
     for b in range(batch_size):
         x_load(b).wait()
 
+    loads[2].start()
+
     def project_kv(j, carry):
         kv_ref[j, device] = jnp.dot(
             x_ref[holder(j)], wkv_ref[...], preferred_element_type=jnp.float32
         ).astype(jnp.bfloat16)
 
+        @pl.when(j == 0)
+        def _():
+            pl.semaphore_wait(
+                barrier,
+                chips + columns - 1
+                + (z > 0).astype(jnp.int32) + (z < rows_z - 1).astype(jnp.int32),
+            )
+
         @pl.when((j == 0) | (z == 0))
         def _():
             send_own(j)
 
         return carry
 
-    lax.fori_loop(0, row_live, project_kv, 0)
+    lax.fori_loop(0, jnp.where(z == 0, 1, row_live), project_kv, 0)
+    loads[3].start()
     loads[2].wait()
-    loads[3].wait()
+    loads[5].wait()
 
     def project_q(j):
         queries = jnp.dot(
@@ -331,6 +339,14 @@
         def _():
             project_q(j)
             attend_own(j)
+
+        @pl.when((z == 0) & (j + 1 < row_live))
+        def _():
+            project_kv(j + 1, 0)
+
+        @pl.when(j == 0)
+        def _():
+            loads[3].wait()
 
         @pl.when((j == 0) & (z > 0))
         def _():
@@ -428,9 +444,11 @@
     return pl.pallas_call(
         functools.partial(layer_kernel, reach, columns, kv_local, per_group, tp),
         out_shape=jax.ShapeDtypeStruct((batch_size, positions, width), bf16),
-        in_specs=[pl.BlockSpec(memory_space=pltpu.SMEM)] + [hbm] * 5 + [vmem],
+        in_specs=[hbm] * 7,
         out_specs=vmem,
         scratch_shapes=[
+            pltpu.SMEM(lengths.shape, jnp.int32),
+            pltpu.VMEM(chosen.shape, jnp.int32),
             pltpu.VMEM(inputs.shape, bf16),
             pltpu.VMEM(query_weight.shape, bf16),
             pltpu.VMEM((model_width, 2 * kv_local * HD), bf16),
@@ -444,7 +462,7 @@
             pair, pair, far, far,
             pltpu.VMEM((steps, STEP_ROWS, width), f32),
             pltpu.VMEM((batch_size, positions, width), bf16),
-            dma((4 + batch_size,)),
+            dma((6 + batch_size,)),
             dma((batch_size, devices // columns, PIECES)),
             dma((batch_size, devices // columns, max(columns - 1, 1), PIECES)),
             dma((batch_size, devices, PIECES)),
@@ -457,13 +475,31 @@
     )(lengths, inputs, query_weight, key_weight, value_weight, out_weight, chosen)
 
 
+def fits_kernel(limits, length_ref, out_ref):
+    lengths = [length_ref[b] for b in range(length_ref.shape[0])]
+    fits = jnp.int32(1)
+    for j, limit in enumerate(limits):
+        longer = sum([(length > limit).astype(jnp.int32) for length in lengths])
+        fits = fits * (longer <= j).astype(jnp.int32)
+    out_ref[0] = fits
+
+
+def fits_short(lengths, limits):
+    smem = pl.BlockSpec(memory_space=pltpu.SMEM)
+    return pl.pallas_call(
+        functools.partial(fits_kernel, limits),
+        out_shape=jax.ShapeDtypeStruct((1,), jnp.int32),
+        in_specs=[smem], out_specs=smem,
+    )(lengths)
+
+
 def shards(*args):
     inputs, lengths = args[0], args[-1]
     batch_size, positions, _ = inputs.shape
     short, whole = spans(batch_size, lax.axis_size("kv"), positions)
-    longer = [jnp.sum(lengths > span * positions) <= j for j, span in enumerate(short)]
+    fits = fits_short(lengths, tuple(span * positions for span in short))
     return lax.cond(
-        functools.reduce(jnp.logical_and, longer),
+        fits[0] > 0,
         functools.partial(layer, short, 0),
         functools.partial(layer, whole, 1),
         *args,

time: 45.3 us -> 42.5 us (0.938)
  between operations: 2.56 us -> 0.67 us
  other arithmetic: 1.38 us -> 0 us
  Pallas kernels: 39.7 us -> 40.2 us
    reduce_sum x1 -> x0, other arithmetic: 1.38 us -> none  [shards(): jnp.sum(lengths > span * positions) <= j]
    pallas_call x0 -> x1, Pallas kernels: none -> 1.2 us  [fits_short(): pl.pallas_call(functools.partial(fits_kernel, limits), out_shape=jax.Shap...]
    pallas_call x1, Pallas kernels: 39.7 us -> 39 us  [layer(): pl.pallas_call(functools.partial(layer_kernel, reach, columns, kv_local,...]
where the time goes in v3:
time: 42.5 us; the launch traced here: 41.9 us
  Pallas kernels  40.2 us (95%)
  local copies, waits for them, and re-layouts  0.97 us (2%)
  between operations  0.67 us (2%)
    pallas_call x1, Pallas kernels, layer(): pl.pallas_call(functools.partial(layer_kernel, reach, columns, kv_local,...  39 us
    pallas_call x1, Pallas kernels, fits_short(): pl.pallas_call(functools.partial(fits_kernel, limits), out_shape=jax.Shap...  1.2 us
    unnamed x1, local copies, waits for them, and re-layouts  0.97 us

profile of v3, /device:TPU:25, one launch (start us, length us, event | category | flops | bytes accessed | tf_op | source)
XLA Modules:
  0.0 41.9 jit_solution(14442611669083458297)
XLA Ops:
  0.0 1.2 %shard_map.75 = s32[1]{0:T(128)} custom-call(s32[4]{0:T(128)} %length_ref.1), custom_call_target="tpu_custom_call" | custom-call | tf_op jit(solution)/shard_map/pallas_call | solution.py:489
  1.9 39.0 %conditional.1 = (bf16[4,256,512]{2,1,0:T(8,128)(2,1)S(1)}) conditional(s32[]{:T(128)} %bitcast, (s32[4]{0:T(128)}, bf16[4,256,2048]{2,1,0:T(8,128)(2,1)}, bf16[2048,512]{1,0:T(8,128)(2,1)}, bf16[2048,256]{1,0:T(8,128)(2,1)}, bf16[2048,256]{1,0:T(8,128)(2,1)}, /*index=5*/bf16[512,2048]{1,0:T(8,128)(2,1)}, s32[4,4,32]{2,1,0:T(4,128)}) %tuple.11, ...), branch_computations={%region_0.0_spmd, %region_1.0_spmd} | conditional | bytes 8 | solution.py:501
  1.9 39.0 %branch_1_fun.1 = bf16[4,256,512]{2,1,0:T(8,128)(2,1)S(1)} custom-call(s32[4]{0:T(128)} %get-tuple-element.43.length_hbm, bf16[4,256,2048]{2,1,0:T(8,128)(2,1)} %get-tuple-element.44.x_hbm, bf16[2048,512]{1,0:T(8,128)(2,1)} %get-tuple-element.45.wq_hbm, bf16[2048,256]{1,0:T(8,128)(2,1)} %get-tuple-element.46.wk_hbm, ...), custom_call_target="tpu_custom_call" | custom-call | tf_op jit(solution)/shard_map/cond/branch_1_fun/pallas_call | solution.py:444
  40.9 1.0 %copy.13 = bf16[4,256,512]{2,1,0:T(8,128)(2,1)} copy(bf16[4,256,512]{2,1,0:T(8,128)(2,1)S(1)} %get-tuple-element.50) | data formatting | bytes 2097152

commit v4 on v3

--- a/solution.py
+++ b/solution.py
@@ -32,7 +32,7 @@
     length_ref, chosen_ref, x_ref, wq_ref, wkv_ref, wo_ref, kv_ref, q_ref,
     top_ref, total_ref, acc_ref, att_ref,
     pair_out, pair_in, far_out, far_in, near, mixed_ref,
-    load_sem, z_sent, x_sent, got, pair_sent, pair_got, far_sent, far_got,
+    load_sem, z_sent, x_sent, aside, got, pair_sent, pair_got, far_sent, far_got,
 ):
     batch_size, positions, _ = x_ref.shape
     slots, devices = kv_ref.shape[:2]
@@ -75,14 +75,10 @@
         pltpu.make_async_copy(wo_hbm, wo_ref, load_sem.at[3]),
         pltpu.make_async_copy(length_hbm, length_ref, load_sem.at[4]),
         pltpu.make_async_copy(chosen_hbm, chosen_ref, load_sem.at[5]),
+        pltpu.make_async_copy(x_hbm, x_ref, load_sem.at[6]),
     ]
-
-    def x_load(b):
-        return pltpu.make_async_copy(x_hbm.at[b], x_ref.at[b], load_sem.at[6 + b])
-
     loads[4].start()
-    for b in range(batch_size):
-        x_load(b).start()
+    loads[6].start()
     loads[0].start()
     loads[1].start()
     loads[5].start()
@@ -119,54 +115,88 @@
     def holder(j):
         return sum([jnp.where(ranks[b] == j, b, 0) for b in range(batch_size)])
 
-    def piece(j, c, p):
-        return kv_ref.at[j, c, pl.ds(p * piece_rows, piece_rows)]
-
-    def z_copy(j, c, p):
+    def at_slot(j, row):
+        return row + sum(
+            [jnp.where(k < j, -(-reach[k] // columns), 0) for k in range(slots - 1)]
+        )
+
+    def part(j, c, p, n):
+        return kv_ref.at[j, c, pl.ds(p * piece_rows, n * piece_rows)]
+
+    def send(j, c, p, n, sent, where):
         return pltpu.make_async_remote_copy(
-            src_ref=piece(j, c, p), dst_ref=piece(j, c, p),
-            send_sem=z_sent.at[j, c // columns, p], recv_sem=got.at[j, c, p],
-            device_id={"kv": device + columns}, device_id_type=MESH,
-        )
-
-    def x_copy(j, c, p, i):
-        return pltpu.make_async_remote_copy(
-            src_ref=piece(j, c, p), dst_ref=piece(j, c, p),
-            send_sem=x_sent.at[j, c // columns, i - 1, p], recv_sem=got.at[j, c, p],
-            device_id={"kv": z * columns + column(i)}, device_id_type=MESH,
-        )
+            src_ref=part(j, c, p, n), dst_ref=part(j, c, p, n), send_sem=sent,
+            recv_sem=got.at[at_slot(j, c // columns), lax.rem(c, columns), p],
+            device_id=where, device_id_type=MESH,
+        )
+
+    def z_copy(j, c, p, n=1):
+        return send(
+            j, c, p, n, z_sent.at[at_slot(j, c // columns)], {"kv": device + columns}
+        )
+
+    def x_copy(j, c, p, i, n=1):
+        return send(
+            j, c, p, n, x_sent.at[at_slot(j, c // columns), i - 1],
+            {"kv": z * columns + column(i)},
+        )
+
+    def aside_copy(j):
+        first = PIECES // 2
+        return send(j, device - 1, first, PIECES - first, aside.at[j], {"kv": device + columns})
 
     def arrival(j, c, p):
-        return pltpu.make_async_remote_copy(
-            src_ref=piece(j, c, p), dst_ref=piece(j, c, p),
-            send_sem=z_sent.at[j, c // columns, p], recv_sem=got.at[j, c, p],
-            device_id={"tp": partner}, device_id_type=MESH,
-        )
-
-    def each_send(j, c, p, act):
+        return send(j, c, p, 1, z_sent.at[at_slot(j, c // columns)], {"tp": partner})
+
+    def by_z(c, i):
+        return (c == device - columns) & (x == 0) & (column(i) == 1)
+
+    def to_row(j, c, i):
         own = c == device
-
+        return (j < live_at(z * columns + column(i))) & (
+            jnp.logical_not(own) | (column(i) > x)
+        )
+
+    def each_send(j, c, p):
         @pl.when(j < next_live)
         def _():
-            act(z_copy(j, c, p))
+            z_copy(j, c, p).start()
 
         for i in range(1, columns):
-            wanted = (j < live_at(z * columns + column(i))) & (
-                jnp.logical_not(own) | (column(i) > x)
-            )
+            wanted = to_row(j, c, i)
+            if p >= PIECES // 2:
+                wanted = wanted & jnp.logical_not(by_z(c, i))
 
             @pl.when(wanted)
             def _():
-                act(x_copy(j, c, p, i))
+                x_copy(j, c, p, i).start()
+
+    def each_sent(j, c):
+        @pl.when(j < next_live)
+        def _():
+            z_copy(j, c, 0, PIECES).wait_send()
+
+        for i in range(1, columns):
+            @pl.when(to_row(j, c, i) & by_z(c, i))
+            def _():
+                x_copy(j, c, 0, i, PIECES // 2).wait_send()
+
+            @pl.when(to_row(j, c, i) & jnp.logical_not(by_z(c, i)))
+            def _():
+                x_copy(j, c, 0, i, PIECES).wait_send()
+
+    def put_aside(j, act):
+        @pl.when((x == 1) & (j < live_at(device + columns)))
+        def _():
+            act(aside_copy(j))
 
     def send_own(j):
         for p in range(PIECES):
-            each_send(j, device, p, lambda copy: copy.start())
+            each_send(j, device, p)
 
     loads[0].wait()
     loads[1].wait()
-    for b in range(batch_size):
-        x_load(b).wait()
+    loads[6].wait()
 
     loads[2].start()
 
@@ -287,7 +317,7 @@
     def pair_copy(i):
         return pltpu.make_async_remote_copy(
             src_ref=pair_out.at[i], dst_ref=pair_in.at[i],
-            send_sem=pair_sent.at[i], recv_sem=pair_got.at[i],
+            send_sem=pair_sent.at[i], recv_sem=pair_got.at[lax.rem(i, 2 * mix_steps)],
             device_id={"tp": partner}, device_id_type=MESH,
         )
 
@@ -325,7 +355,7 @@
 
         for p in range(PIECES):
             arrival(j, c, p).wait_recv()
-            each_send(j, c, p, lambda copy: copy.start())
+            each_send(j, c, p)
 
     def take(j, c):
         for p in range(PIECES):
@@ -355,24 +385,37 @@
         def step(t, carry):
             d = t // columns
             i = lax.rem(t, columns)
-            c = (z - d) * columns + column(i)
             ahead = j * z + d
-
-            @pl.when((i == 0) & (d > 0) & (ahead < row_live * z))
+            below = (i == 0) & (d > 0) & (d <= z)
+
+            @pl.when((z > 0) & (i == 0) & (d == jnp.maximum(z, 2)))
+            def _():
+                put_aside(j, lambda copy: copy.start())
+
+            @pl.when(below & (ahead < row_live * z))
             def _():
                 relay(ahead)
 
-            @pl.when(used & (i == 0) & (d > 0))
-            def _():
-                attend_far(j, c)
-
-            @pl.when(used & (i > 0) & ((d > 0) | (column(i) < x)))
-            def _():
-                take(j, c)
+            @pl.when(used & below)
+            def _():
+                attend_far(j, device - d * columns)
+
+            other = column(i)
+            late = (x == 1) & (other == 0)
+            last = d - 1
+            back = jnp.where(late & (last > 0), lax.rem(last, jnp.maximum(z, 1)) + 1, last)
+
+            @pl.when(used & (i > 0) & (d > 0) & ((last > 0) | (other < x)))
+            def _():
+                take(j, (z - back) * columns + other)
 
             return carry
 
-        lax.fori_loop(0, (z + 1) * columns, step, 0)
+        lax.fori_loop(0, (z + 2) * columns, step, 0)
+
+        @pl.when(z == 0)
+        def _():
+            put_aside(j, lambda copy: copy.start())
 
         @pl.when(used)
         def _():
@@ -407,10 +450,10 @@
     def drain(j, carry):
         def back(d, carry):
             c = (z - d) * columns + x
-            for p in range(PIECES):
-                each_send(j, c, p, lambda copy: copy.wait_send())
+            each_sent(j, c)
             return carry
 
+        put_aside(j, lambda copy: copy.wait_send())
         return lax.fori_loop(0, z + 1, back, carry)
 
     lax.fori_loop(0, row_live, drain, 0)
@@ -435,6 +478,7 @@
     width = out_weight.shape[1] // tp
     steps = batch_size * (positions // STEP_ROWS)
     rows = per_group * positions
+    reached = sum([-(-span // columns) for span in reach])
     bf16, f32 = jnp.bfloat16, jnp.float32
     vmem = pl.BlockSpec(memory_space=pltpu.VMEM)
     hbm = pl.BlockSpec(memory_space=pl.ANY)
@@ -462,11 +506,12 @@
             pair, pair, far, far,
             pltpu.VMEM((steps, STEP_ROWS, width), f32),
             pltpu.VMEM((batch_size, positions, width), bf16),
-            dma((6 + batch_size,)),
-            dma((batch_size, devices // columns, PIECES)),
-            dma((batch_size, devices // columns, max(columns - 1, 1), PIECES)),
-            dma((batch_size, devices, PIECES)),
-            dma((steps,)), dma((steps,)),
+            dma((7,)),
+            dma((reached,)),
+            dma((reached, max(columns - 1, 1))),
+            dma((batch_size,)),
+            dma((reached, columns, PIECES)),
+            dma((steps,)), dma((2 * (positions // STEP_ROWS),)),
             dma((chips - 1, steps)), dma((chips - 1, steps)),
         ],
         compiler_params=pltpu.CompilerParams(

time: 42.5 us -> 41.3 us (0.972); the launches traced: 41.9 us -> 41.2 us
  Pallas kernels: 40.2 us -> 39.5 us
    pallas_call x1, Pallas kernels: 39 us -> 38.3 us  [layer(): pl.pallas_call(functools.partial(layer_kernel, reach, columns, kv_local,...]
where the time goes in v4:
time: 41.3 us; the launch traced here: 41.2 us
  Pallas kernels  39.5 us (96%)
  local copies, waits for them, and re-layouts  0.97 us (2%)
  between operations  0.67 us (2%)
    pallas_call x1, Pallas kernels, layer(): pl.pallas_call(functools.partial(layer_kernel, reach, columns, kv_local,...  38.3 us
    pallas_call x1, Pallas kernels, fits_short(): pl.pallas_call(functools.partial(fits_kernel, limits), out_shape=jax.Shap...  1.2 us
    unnamed x1, local copies, waits for them, and re-layouts  0.97 us

profile of v4, /device:TPU:25, one launch (start us, length us, event | category | flops | bytes accessed | tf_op | source)
XLA Modules:
  0.0 41.2 jit_solution(3873254009267874217)
XLA Ops:
  0.0 1.2 %shard_map.75 = s32[1]{0:T(128)} custom-call(s32[4]{0:T(128)} %length_ref.1), custom_call_target="tpu_custom_call" | custom-call | tf_op jit(solution)/shard_map/pallas_call | solution.py:534
  1.9 38.3 %conditional.1 = (bf16[4,256,512]{2,1,0:T(8,128)(2,1)S(1)}) conditional(s32[]{:T(128)} %bitcast, (s32[4]{0:T(128)}, bf16[4,256,2048]{2,1,0:T(8,128)(2,1)}, bf16[2048,512]{1,0:T(8,128)(2,1)}, bf16[2048,256]{1,0:T(8,128)(2,1)}, bf16[2048,256]{1,0:T(8,128)(2,1)}, /*index=5*/bf16[512,2048]{1,0:T(8,128)(2,1)}, s32[4,4,32]{2,1,0:T(4,128)}) %tuple.11, ...), branch_computations={%region_0.0_spmd, %region_1.0_spmd} | conditional | bytes 8 | solution.py:546
  1.9 38.3 %branch_1_fun.1 = bf16[4,256,512]{2,1,0:T(8,128)(2,1)S(1)} custom-call(s32[4]{0:T(128)} %get-tuple-element.43.length_hbm, bf16[4,256,2048]{2,1,0:T(8,128)(2,1)} %get-tuple-element.44.x_hbm, bf16[2048,512]{1,0:T(8,128)(2,1)} %get-tuple-element.45.wq_hbm, bf16[2048,256]{1,0:T(8,128)(2,1)} %get-tuple-element.46.wk_hbm, ...), custom_call_target="tpu_custom_call" | custom-call | tf_op jit(solution)/shard_map/cond/branch_1_fun/pallas_call | solution.py:488
  40.2 1.0 %copy.13 = bf16[4,256,512]{2,1,0:T(8,128)(2,1)} copy(bf16[4,256,512]{2,1,0:T(8,128)(2,1)S(1)} %get-tuple-element.50) | data formatting | bytes 2097152

commit v5 on v4

--- a/solution.py
+++ b/solution.py
@@ -28,8 +28,8 @@
 
 def layer_kernel(
     reach, columns, kv_local, per_group, tp,
-    length_hbm, x_hbm, wq_hbm, wk_hbm, wv_hbm, wo_hbm, chosen_hbm, out_ref,
-    length_ref, chosen_ref, x_ref, wq_ref, wkv_ref, wo_ref, kv_ref, q_ref,
+    slot_ref, x_ref, wkv_ref, wq_hbm, wo_hbm, chosen_hbm, out_ref,
+    chosen_ref, wq_ref, wo_ref, kv_ref, q_ref,
     top_ref, total_ref, acc_ref, att_ref,
     pair_out, pair_in, far_out, far_in, near, mixed_ref,
     load_sem, z_sent, x_sent, aside, got, pair_sent, pair_got, far_sent, far_got,
@@ -69,19 +69,12 @@
     next_live = live_at((z + 1) * columns)
 
     loads = [
-        pltpu.make_async_copy(wk_hbm, wkv_ref.at[:, pl.ds(0, half)], load_sem.at[0]),
-        pltpu.make_async_copy(wv_hbm, wkv_ref.at[:, pl.ds(half, half)], load_sem.at[1]),
-        pltpu.make_async_copy(wq_hbm, wq_ref, load_sem.at[2]),
-        pltpu.make_async_copy(wo_hbm, wo_ref, load_sem.at[3]),
-        pltpu.make_async_copy(length_hbm, length_ref, load_sem.at[4]),
-        pltpu.make_async_copy(chosen_hbm, chosen_ref, load_sem.at[5]),
-        pltpu.make_async_copy(x_hbm, x_ref, load_sem.at[6]),
+        pltpu.make_async_copy(wq_hbm, wq_ref, load_sem.at[0]),
+        pltpu.make_async_copy(chosen_hbm, chosen_ref, load_sem.at[1]),
+        pltpu.make_async_copy(wo_hbm, wo_ref, load_sem.at[2]),
     ]
-    loads[4].start()
-    loads[6].start()
-    loads[0].start()
-    loads[1].start()
-    loads[5].start()
+    for load in loads:
+        load.start()
 
     barrier = pltpu.get_barrier_semaphore()
 
@@ -102,18 +95,8 @@
     def _():
         greet(kv=device + columns)
 
-    loads[4].wait()
-    lengths = [length_ref[b] for b in range(batch_size)]
-    ranks = []
-    for b in range(batch_size):
-        ahead = [
-            (lengths[o] >= lengths[b] if o < b else lengths[o] > lengths[b]).astype(jnp.int32)
-            for o in range(batch_size) if o != b
-        ]
-        ranks.append(sum(ahead))
-
     def holder(j):
-        return sum([jnp.where(ranks[b] == j, b, 0) for b in range(batch_size)])
+        return slot_ref[1 + j]
 
     def at_slot(j, row):
         return row + sum(
@@ -194,15 +177,9 @@
         for p in range(PIECES):
             each_send(j, device, p)
 
-    loads[0].wait()
-    loads[1].wait()
-    loads[6].wait()
-
-    loads[2].start()
-
     def project_kv(j, carry):
         kv_ref[j, device] = jnp.dot(
-            x_ref[holder(j)], wkv_ref[...], preferred_element_type=jnp.float32
+            x_ref[j], wkv_ref[...], preferred_element_type=jnp.float32
         ).astype(jnp.bfloat16)
 
         @pl.when(j == 0)
@@ -220,13 +197,12 @@
         return carry
 
     lax.fori_loop(0, jnp.where(z == 0, 1, row_live), project_kv, 0)
-    loads[3].start()
-    loads[2].wait()
-    loads[5].wait()
+    loads[0].wait()
+    loads[1].wait()
 
     def project_q(j):
         queries = jnp.dot(
-            x_ref[holder(j)], wq_ref[...], preferred_element_type=jnp.float32
+            x_ref[j], wq_ref[...], preferred_element_type=jnp.float32
         ).astype(jnp.bfloat16)
         for n in range(kv_local * per_group):
             h, g = n // per_group, n % per_group
@@ -294,9 +270,7 @@
             acc_ref[h] = acc_ref[h] * fade + weigh(j, c, h, raised)
 
     def attend_end(j):
-        live = sum(
-            [jnp.where(ranks[b] == j, lengths[b], 0) for b in range(batch_size)]
-        ) - device * positions
+        live = slot_ref[1 + 2 * batch_size + j] - device * positions
         living = lax.broadcasted_iota(jnp.int32, (positions, HD), 0) < live
         for h in range(kv_local):
             done = acc_ref[h] / total_ref[h]
@@ -376,7 +350,7 @@
 
         @pl.when(j == 0)
         def _():
-            loads[3].wait()
+            loads[2].wait()
 
         @pl.when((j == 0) & (z > 0))
         def _():
@@ -445,7 +419,7 @@
 
     lax.fori_loop(mine, slots, blank, 0)
     for b in range(batch_size):
-        out_ref[b] = mixed_ref[ranks[b]]
+        out_ref[b] = mixed_ref[slot_ref[1 + batch_size + b]]
 
     def drain(j, carry):
         def back(d, carry):
@@ -464,11 +438,11 @@
 
 
 def layer(
-    reach, collective_id,
-    inputs, query_weight, key_weight, value_weight, out_weight, chosen, lengths,
+    reach, collective_id, slot, x, key_value_weight,
+    query_weight, out_weight, chosen,
 ):
-    batch_size, positions, model_width = inputs.shape
-    kv_local = key_weight.shape[1] // HD
+    batch_size, positions, _ = x.shape
+    kv_local = key_value_weight.shape[1] // (2 * HD)
     heads_local = query_weight.shape[1] // HD
     per_group = heads_local // kv_local
     devices = lax.axis_size("kv")
@@ -481,6 +455,7 @@
     reached = sum([-(-span // columns) for span in reach])
     bf16, f32 = jnp.bfloat16, jnp.float32
     vmem = pl.BlockSpec(memory_space=pltpu.VMEM)
+    smem = pl.BlockSpec(memory_space=pltpu.SMEM)
     hbm = pl.BlockSpec(memory_space=pl.ANY)
     dma = pltpu.SemaphoreType.DMA
     pair = pltpu.VMEM((steps, chips, STEP_ROWS, width), bf16)
@@ -488,14 +463,11 @@
     return pl.pallas_call(
         functools.partial(layer_kernel, reach, columns, kv_local, per_group, tp),
         out_shape=jax.ShapeDtypeStruct((batch_size, positions, width), bf16),
-        in_specs=[hbm] * 7,
+        in_specs=[smem, vmem, vmem, hbm, hbm, hbm],
         out_specs=vmem,
         scratch_shapes=[
-            pltpu.SMEM(lengths.shape, jnp.int32),
             pltpu.VMEM(chosen.shape, jnp.int32),
-            pltpu.VMEM(inputs.shape, bf16),
             pltpu.VMEM(query_weight.shape, bf16),
-            pltpu.VMEM((model_width, 2 * kv_local * HD), bf16),
             pltpu.VMEM(out_weight.shape, bf16),
             pltpu.VMEM((batch_size, devices, positions, 2 * kv_local * HD), bf16),
             pltpu.VMEM((kv_local, rows, HD), bf16),
@@ -506,7 +478,7 @@
             pair, pair, far, far,
             pltpu.VMEM((steps, STEP_ROWS, width), f32),
             pltpu.VMEM((batch_size, positions, width), bf16),
-            dma((7,)),
+            dma((3,)),
             dma((reached,)),
             dma((reached, max(columns - 1, 1))),
             dma((batch_size,)),
@@ -515,39 +487,91 @@
             dma((chips - 1, steps)), dma((chips - 1, steps)),
         ],
         compiler_params=pltpu.CompilerParams(
-            collective_id=collective_id, has_side_effects=True, vmem_limit_bytes=60 * 2**20
+            collective_id=collective_id, has_side_effects=True, vmem_limit_bytes=56 * 2**20
         ),
-    )(lengths, inputs, query_weight, key_weight, value_weight, out_weight, chosen)
-
-
-def fits_kernel(limits, length_ref, out_ref):
-    lengths = [length_ref[b] for b in range(length_ref.shape[0])]
+    )(slot, x, key_value_weight, query_weight, out_weight, chosen)
+
+
+def prepare_kernel(
+    short, whole, columns, length_hbm, x_hbm, wk_hbm, wv_hbm,
+    slot_ref, x_ref, wkv_ref, length_ref, load_sem,
+):
+    batch_size, positions, _ = x_ref.shape
+    half = wkv_ref.shape[1] // 2
+    first = lax.axis_index("kv") // columns * columns
+    loads = [
+        pltpu.make_async_copy(length_hbm, length_ref, load_sem.at[0]),
+        pltpu.make_async_copy(wk_hbm, wkv_ref.at[:, pl.ds(0, half)], load_sem.at[1]),
+        pltpu.make_async_copy(wv_hbm, wkv_ref.at[:, pl.ds(half, half)], load_sem.at[2]),
+    ]
+    for load in loads:
+        load.start()
+    loads[0].wait()
+
+    lengths = [length_ref[b] for b in range(batch_size)]
+    ranks = []
+    for b in range(batch_size):
+        ahead = [
+            (lengths[o] >= lengths[b] if o < b else lengths[o] > lengths[b]).astype(jnp.int32)
+            for o in range(batch_size) if o != b
+        ]
+        ranks.append(sum(ahead))
+    slots = range(batch_size)
+    held = [sum([jnp.where(ranks[b] == j, b, 0) for b in slots]) for j in slots]
+    spans = [sum([jnp.where(ranks[b] == j, lengths[b], 0) for b in slots]) for j in slots]
     fits = jnp.int32(1)
-    for j, limit in enumerate(limits):
-        longer = sum([(length > limit).astype(jnp.int32) for length in lengths])
-        fits = fits * (longer <= j).astype(jnp.int32)
-    out_ref[0] = fits
-
-
-def fits_short(lengths, limits):
+    for j in slots:
+        fits = fits * (spans[j] <= short[j] * positions).astype(jnp.int32)
+
+    def x_load(j):
+        return pltpu.make_async_copy(x_hbm.at[held[j]], x_ref.at[j], load_sem.at[3 + j])
+
+    used = [first < jnp.where(fits > 0, short[j], whole[j]) for j in slots]
+    for j in slots:
+        @pl.when(used[j])
+        def _():
+            x_load(j).start()
+
+    slot_ref[0] = fits
+    for j in slots:
+        slot_ref[1 + j] = held[j]
+        slot_ref[1 + batch_size + j] = ranks[j]
+        slot_ref[1 + 2 * batch_size + j] = spans[j]
+    loads[1].wait()
+    loads[2].wait()
+    for j in slots:
+        @pl.when(used[j])
+        def _():
+            x_load(j).wait()
+
+
+def shards(inputs, query_weight, key_weight, value_weight, out_weight, chosen, lengths):
+    batch_size, positions, model_width = inputs.shape
+    devices = lax.axis_size("kv")
+    short, whole = spans(batch_size, devices, positions)
+    hbm = pl.BlockSpec(memory_space=pl.ANY)
+    vmem = pl.BlockSpec(memory_space=pltpu.VMEM)
     smem = pl.BlockSpec(memory_space=pltpu.SMEM)
-    return pl.pallas_call(
-        functools.partial(fits_kernel, limits),
-        out_shape=jax.ShapeDtypeStruct((1,), jnp.int32),
-        in_specs=[smem], out_specs=smem,
-    )(lengths)
-
-
-def shards(*args):
-    inputs, lengths = args[0], args[-1]
-    batch_size, positions, _ = inputs.shape
-    short, whole = spans(batch_size, lax.axis_size("kv"), positions)
-    fits = fits_short(lengths, tuple(span * positions for span in short))
+    slot, x, key_value_weight = pl.pallas_call(
+        functools.partial(prepare_kernel, short, whole, columns_of(devices)),
+        out_shape=(
+            pltpu.SMEM((1 + 3 * batch_size,), jnp.int32),
+            pltpu.VMEM(inputs.shape, inputs.dtype),
+            pltpu.VMEM((model_width, 2 * key_weight.shape[1]), key_weight.dtype),
+        ),
+        in_specs=[hbm] * 4,
+        out_specs=(smem, vmem, vmem),
+        scratch_shapes=[
+            pltpu.SMEM(lengths.shape, jnp.int32),
+            pltpu.SemaphoreType.DMA((3 + batch_size,)),
+        ],
+        compiler_params=pltpu.CompilerParams(vmem_limit_bytes=57 * 2**20),
+    )(lengths, inputs, key_weight, value_weight)
     return lax.cond(
-        fits[0] > 0,
+        slot[0] > 0,
         functools.partial(layer, short, 0),
         functools.partial(layer, whole, 1),
-        *args,
+        slot, x, key_value_weight, query_weight, out_weight, chosen,
     )
 
 

time: 41.3 us -> 39.8 us (0.964)
  Pallas kernels: 39.5 us -> 38.7 us
  between operations: 0.67 us -> 0.03 us
    pallas_call x1, Pallas kernels: 38.3 us -> 36.4 us  [layer(): pl.pallas_call(functools.partial(layer_kernel, reach, columns, kv_local,...]
    pallas_call x1, Pallas kernels: 1.2 us -> 2.26 us  [shards(): pl.pallas_call(functools.partial(prepare_kernel, short, whole, columns_of...]
    unnamed x1 -> x3, local copies, waits for them, and re-layouts: 0.97 us -> 0.98 us
where the time goes in v5:
time: 39.8 us; the launch traced here: 39.7 us
  Pallas kernels  38.7 us (97%)
  local copies, waits for them, and re-layouts  0.98 us (2%)
    pallas_call x1, Pallas kernels, layer(): pl.pallas_call(functools.partial(layer_kernel, reach, columns, kv_local,...  36.4 us
    pallas_call x1, Pallas kernels, shards(): pl.pallas_call(functools.partial(prepare_kernel, short, whole, columns_of...  2.26 us
    unnamed x3, local copies, waits for them, and re-layouts  0.98 us

profile of v5, /device:TPU:25, one launch (start us, length us, event | category | flops | bytes accessed | tf_op | source)
XLA Modules:
  0.0 39.7 jit_solution(423816310113556533)
XLA Ops:
  0.0 0.0 copy-start
  0.0 2.3 %shard_map.75 = (s32[13]{0:T(128)S(4)}, bf16[4,256,2048]{2,1,0:T(8,128)(2,1)S(1)}, bf16[2048,512]{1,0:T(8,128)(2,1)S(1)}) custom-call(s32[4]{0:T(128)} %length_hbm.1, bf16[4,256,2048]{2,1,0:T(8,128)(2,1)} %x_hbm.1, bf16[2048,256]{1,0:T(8,128)(2,1)} %wk_hbm.1, bf16[2048,256]{1,0:T(8,128)(2,1)} %wv_hbm.1), custom_call_target="tpu_custom_call" | custom-call | tf_op jit(solution)/shard_map/pallas_call | solution.py:555
  2.3 0.0 copy-done
  2.3 36.4 %conditional.1 = (bf16[4,256,512]{2,1,0:T(8,128)(2,1)S(1)}) conditional(s32[]{:T(128)} %bitcast, (s32[13]{0:T(128)S(4)}, bf16[4,256,2048]{2,1,0:T(8,128)(2,1)S(1)}, bf16[2048,512]{1,0:T(8,128)(2,1)S(1)}, bf16[2048,512]{1,0:T(8,128)(2,1)}, bf16[512,2048]{1,0:T(8,128)(2,1)}, /*index=5*/s32[4,4,32]{2,1,0:T(4,128)S(1)}) %tuple.16, (s32[13]{0:T(128)S(4)}, ...), branch_computations={%region_0.0_spmd, %region_1.0_spmd} | conditional | bytes 8 | solution.py:570
  2.3 36.4 %branch_1_fun.1 = bf16[4,256,512]{2,1,0:T(8,128)(2,1)S(1)} custom-call(s32[13]{0:T(128)S(4)} %get-tuple-element.38.slot_ref, bf16[4,256,2048]{2,1,0:T(8,128)(2,1)S(1)} %get-tuple-element.39.x_ref, bf16[2048,512]{1,0:T(8,128)(2,1)S(1)} %get-tuple-element.40.wkv_ref, bf16[2048,512]{1,0:T(8,128)(2,1)} %get-tuple-element.41.wq_hbm, ...), custom_call_target="tpu_custom_call" | custom-call | tf_op jit(solution)/shard_map/cond/branch_1_fun/pallas_call | solution.py:463
  38.7 1.0 %copy.13 = bf16[4,256,512]{2,1,0:T(8,128)(2,1)} copy(bf16[4,256,512]{2,1,0:T(8,128)(2,1)S(1)} %get-tuple-element.50) | data formatting | bytes 2097152
Async XLA Ops:
  0.0 2.3 %copy-start = (s32[4,4,32]{2,1,0:T(4,128)S(1)}, s32[4,4,32]{2,1,0:T(4,128)}, u32[]{:S(2)}) copy-start(s32[4,4,32]{2,1,0:T(4,128)} %param.14) | copy-start | bytes 6148

commit v6 on v5

--- a/solution.py
+++ b/solution.py
@@ -10,7 +10,7 @@
 HD = 128
 KB = 64
 MASKED = -1e30
-PIECES = 2
+PIECES = 4
 STEP_ROWS = 128
 MESH = pl.DeviceIdType.MESH
 
@@ -32,7 +32,7 @@
     chosen_ref, wq_ref, wo_ref, kv_ref, q_ref,
     top_ref, total_ref, acc_ref, att_ref,
     pair_out, pair_in, far_out, far_in, near, mixed_ref,
-    load_sem, z_sent, x_sent, aside, got, pair_sent, pair_got, far_sent, far_got,
+    load_sem, z_sent, x_sent, aside, z_got, x_got, pair_sent, pair_got, far_sent, far_got,
 ):
     batch_size, positions, _ = x_ref.shape
     slots, devices = kv_ref.shape[:2]
@@ -106,30 +106,37 @@
     def part(j, c, p, n):
         return kv_ref.at[j, c, pl.ds(p * piece_rows, n * piece_rows)]
 
-    def send(j, c, p, n, sent, where):
+    def send(j, c, p, n, sent, landed, where):
         return pltpu.make_async_remote_copy(
             src_ref=part(j, c, p, n), dst_ref=part(j, c, p, n), send_sem=sent,
-            recv_sem=got.at[at_slot(j, c // columns), lax.rem(c, columns), p],
-            device_id=where, device_id_type=MESH,
+            recv_sem=landed, device_id=where, device_id_type=MESH,
         )
 
     def z_copy(j, c, p, n=1):
+        at = at_slot(j, c // columns)
+        return send(j, c, p, n, z_sent.at[at], z_got.at[at, p], {"kv": device + columns})
+
+    def x_copy(j, c, p, i, n=1):
+        at = at_slot(j, c // columns)
         return send(
-            j, c, p, n, z_sent.at[at_slot(j, c // columns)], {"kv": device + columns}
-        )
-
-    def x_copy(j, c, p, i, n=1):
-        return send(
-            j, c, p, n, x_sent.at[at_slot(j, c // columns), i - 1],
+            j, c, p, n, x_sent.at[at, i - 1], x_got.at[at, columns - i - 1],
             {"kv": z * columns + column(i)},
         )
 
     def aside_copy(j):
         first = PIECES // 2
-        return send(j, device - 1, first, PIECES - first, aside.at[j], {"kv": device + columns})
-
-    def arrival(j, c, p):
-        return send(j, c, p, 1, z_sent.at[at_slot(j, c // columns)], {"tp": partner})
+        return send(
+            j, device - 1, first, PIECES - first, aside.at[j],
+            x_got.at[at_slot(j, z), columns - 2], {"kv": device + columns},
+        )
+
+    def z_arrival(j, c, p):
+        at = at_slot(j, c // columns)
+        return send(j, c, p, 1, z_sent.at[at], z_got.at[at, p], {"tp": partner})
+
+    def x_arrival(j, c, i):
+        at = at_slot(j, c // columns)
+        return send(j, c, 0, PIECES, z_sent.at[at], x_got.at[at, i - 1], {"tp": partner})
 
     def by_z(c, i):
         return (c == device - columns) & (x == 0) & (column(i) == 1)
@@ -318,7 +325,7 @@
                 far_copy(i, off).start()
             near[i] = sums[0] + pair_in[i, 0].astype(jnp.float32)
 
-    def relay(t):
+    def relay(t, between=None):
         j = t // z
         d = lax.rem(t, z)
         c = device - (d + 1) * columns
@@ -328,12 +335,13 @@
             send_own(j)
 
         for p in range(PIECES):
-            arrival(j, c, p).wait_recv()
+            z_arrival(j, c, p).wait_recv()
             each_send(j, c, p)
-
-    def take(j, c):
-        for p in range(PIECES):
-            arrival(j, c, p).wait_recv()
+            if p == 0 and between is not None:
+                between()
+
+    def take(j, c, i):
+        x_arrival(j, c, i).wait_recv()
         attend_far(j, c)
 
     def slot(j, carry):
@@ -366,22 +374,28 @@
             def _():
                 put_aside(j, lambda copy: copy.start())
 
+            def attend_below():
+                @pl.when(used)
+                def _():
+                    attend_far(j, device - d * columns)
+
             @pl.when(below & (ahead < row_live * z))
             def _():
-                relay(ahead)
-
-            @pl.when(used & below)
+                relay(ahead, attend_below)
+
+            @pl.when(below & (ahead >= row_live * z))
             def _():
-                attend_far(j, device - d * columns)
+                attend_below()
 
             other = column(i)
             late = (x == 1) & (other == 0)
             last = d - 1
-            back = jnp.where(late & (last > 0), lax.rem(last, jnp.maximum(z, 1)) + 1, last)
+            turn = jnp.where(last == z, z, jnp.where(last == z - 1, 1, last + 1))
+            back = jnp.where(late & (last > 0), turn, last)
 
             @pl.when(used & (i > 0) & (d > 0) & ((last > 0) | (other < x)))
             def _():
-                take(j, (z - back) * columns + other)
+                take(j, (z - back) * columns + other, jnp.maximum(i, 1))
 
             return carry
 
@@ -482,7 +496,8 @@
             dma((reached,)),
             dma((reached, max(columns - 1, 1))),
             dma((batch_size,)),
-            dma((reached, columns, PIECES)),
+            dma((reached, PIECES)),
+            dma((reached, max(columns - 1, 1))),
             dma((steps,)), dma((2 * (positions // STEP_ROWS),)),
             dma((chips - 1, steps)), dma((chips - 1, steps)),
         ],

time: 39.8 us -> 39.2 us (0.985)
  Pallas kernels: 38.7 us -> 38 us
    pallas_call x1, Pallas kernels: 36.4 us -> 35.8 us  [layer(): pl.pallas_call(functools.partial(layer_kernel, reach, columns, kv_local,...]
where the time goes in v6:
time: 39.2 us; the launch traced here: 39.1 us
  Pallas kernels  38 us (97%)
  local copies, waits for them, and re-layouts  0.98 us (2%)
    pallas_call x1, Pallas kernels, layer(): pl.pallas_call(functools.partial(layer_kernel, reach, columns, kv_local,...  35.8 us
    pallas_call x1, Pallas kernels, shards(): pl.pallas_call(functools.partial(prepare_kernel, short, whole, columns_of...  2.26 us
    unnamed x3, local copies, waits for them, and re-layouts  0.98 us

profile of v6, /device:TPU:25, one launch (start us, length us, event | category | flops | bytes accessed | tf_op | source)
XLA Modules:
  0.0 39.1 jit_solution(1440174607568022028)
XLA Ops:
  0.0 0.0 copy-start
  0.0 2.3 %shard_map.75 = (s32[13]{0:T(128)S(4)}, bf16[4,256,2048]{2,1,0:T(8,128)(2,1)S(1)}, bf16[2048,512]{1,0:T(8,128)(2,1)S(1)}) custom-call(s32[4]{0:T(128)} %length_hbm.1, bf16[4,256,2048]{2,1,0:T(8,128)(2,1)} %x_hbm.1, bf16[2048,256]{1,0:T(8,128)(2,1)} %wk_hbm.1, bf16[2048,256]{1,0:T(8,128)(2,1)} %wv_hbm.1), custom_call_target="tpu_custom_call" | custom-call | tf_op jit(solution)/shard_map/pallas_call | solution.py:570
  2.3 0.0 copy-done
  2.3 35.8 %conditional.1 = (bf16[4,256,512]{2,1,0:T(8,128)(2,1)S(1)}) conditional(s32[]{:T(128)} %bitcast, (s32[13]{0:T(128)S(4)}, bf16[4,256,2048]{2,1,0:T(8,128)(2,1)S(1)}, bf16[2048,512]{1,0:T(8,128)(2,1)S(1)}, bf16[2048,512]{1,0:T(8,128)(2,1)}, bf16[512,2048]{1,0:T(8,128)(2,1)}, /*index=5*/s32[4,4,32]{2,1,0:T(4,128)S(1)}) %tuple.16, (s32[13]{0:T(128)S(4)}, ...), branch_computations={%region_0.0_spmd, %region_1.0_spmd} | conditional | bytes 8 | solution.py:585
  2.3 35.8 %branch_1_fun.1 = bf16[4,256,512]{2,1,0:T(8,128)(2,1)S(1)} custom-call(s32[13]{0:T(128)S(4)} %get-tuple-element.38.slot_ref, bf16[4,256,2048]{2,1,0:T(8,128)(2,1)S(1)} %get-tuple-element.39.x_ref, bf16[2048,512]{1,0:T(8,128)(2,1)S(1)} %get-tuple-element.40.wkv_ref, bf16[2048,512]{1,0:T(8,128)(2,1)} %get-tuple-element.41.wq_hbm, ...), custom_call_target="tpu_custom_call" | custom-call | tf_op jit(solution)/shard_map/cond/branch_1_fun/pallas_call | solution.py:477
  38.1 1.0 %copy.13 = bf16[4,256,512]{2,1,0:T(8,128)(2,1)} copy(bf16[4,256,512]{2,1,0:T(8,128)(2,1)S(1)} %get-tuple-element.50) | data formatting | bytes 2097152
Async XLA Ops:
  0.0 2.3 %copy-start = (s32[4,4,32]{2,1,0:T(4,128)S(1)}, s32[4,4,32]{2,1,0:T(4,128)}, u32[]{:S(2)}) copy-start(s32[4,4,32]{2,1,0:T(4,128)} %param.14) | copy-start | bytes 6148

commit v7 on v6

--- a/solution.py
+++ b/solution.py
@@ -223,6 +223,9 @@
                 jnp.where(names == c * per_dev + i, 0.0, MASKED), axis=1, keepdims=True
             )
             bias = jnp.where(segment == i, hit, bias)
+        return bias
+
+    def by_row(bias):
         return jnp.broadcast_to(bias[:, None, :], (per_dev, KB, positions)).reshape(
             positions, positions
         )
@@ -246,7 +249,7 @@
 
     def attend_own(j):
         names = chosen_ref[holder(j)]
-        before = named(names, device)
+        before = by_row(named(names, device))
         home = device * per_dev + lax.broadcasted_iota(jnp.int32, names.shape, 0)
         copies = jnp.sum(jnp.where(names == home, 1.0, 0.0), axis=1, keepdims=True)
         same = jnp.log(jnp.maximum(copies, 1.0))
@@ -264,8 +267,11 @@
             total_ref[h] = jnp.broadcast_to(jnp.sum(raised, axis=1, keepdims=True), (rows, HD))
             acc_ref[h] = weigh(j, device, h, raised)
 
-    def attend_far(j, c):
+    def attend_far(j, c, arrive=None):
         bias = named(chosen_ref[holder(j)], c)
+        if arrive is not None:
+            arrive()
+        bias = by_row(bias)
         for h in range(kv_local):
             s = scores(j, c, h, bias)
             old = top_ref[h]
@@ -341,8 +347,7 @@
                 between()
 
     def take(j, c, i):
-        x_arrival(j, c, i).wait_recv()
-        attend_far(j, c)
+        attend_far(j, c, lambda: x_arrival(j, c, i).wait_recv())
 
     def slot(j, carry):
         used = j < mine

time: 39.2 us -> 39.2 us (level)
  no operation moved by 1% of the time
where the time goes in v7:
time: 39.2 us; the launch traced here: 39.1 us
  Pallas kernels  38 us (97%)
  local copies, waits for them, and re-layouts  0.98 us (2%)
    pallas_call x1, Pallas kernels, layer(): pl.pallas_call(functools.partial(layer_kernel, reach, columns, kv_local,...  35.8 us
    pallas_call x1, Pallas kernels, shards(): pl.pallas_call(functools.partial(prepare_kernel, short, whole, columns_of...  2.26 us
    unnamed x3, local copies, waits for them, and re-layouts  0.98 us

profile of v7, /device:TPU:25, one launch (start us, length us, event | category | flops | bytes accessed | tf_op | source)
XLA Modules:
  0.0 39.1 jit_solution(17843334224535992210)
XLA Ops:
  0.0 0.0 copy-start
  0.0 2.3 %shard_map.75 = (s32[13]{0:T(128)S(4)}, bf16[4,256,2048]{2,1,0:T(8,128)(2,1)S(1)}, bf16[2048,512]{1,0:T(8,128)(2,1)S(1)}) custom-call(s32[4]{0:T(128)} %length_hbm.1, bf16[4,256,2048]{2,1,0:T(8,128)(2,1)} %x_hbm.1, bf16[2048,256]{1,0:T(8,128)(2,1)} %wk_hbm.1, bf16[2048,256]{1,0:T(8,128)(2,1)} %wv_hbm.1), custom_call_target="tpu_custom_call" | custom-call | tf_op jit(solution)/shard_map/pallas_call | solution.py:575
  2.3 0.0 copy-done
  2.3 35.8 %conditional.1 = (bf16[4,256,512]{2,1,0:T(8,128)(2,1)S(1)}) conditional(s32[]{:T(128)} %bitcast, (s32[13]{0:T(128)S(4)}, bf16[4,256,2048]{2,1,0:T(8,128)(2,1)S(1)}, bf16[2048,512]{1,0:T(8,128)(2,1)S(1)}, bf16[2048,512]{1,0:T(8,128)(2,1)}, bf16[512,2048]{1,0:T(8,128)(2,1)}, /*index=5*/s32[4,4,32]{2,1,0:T(4,128)S(1)}) %tuple.16, (s32[13]{0:T(128)S(4)}, ...), branch_computations={%region_0.0_spmd, %region_1.0_spmd} | conditional | bytes 8 | solution.py:590
  2.3 35.8 %branch_1_fun.1 = bf16[4,256,512]{2,1,0:T(8,128)(2,1)S(1)} custom-call(s32[13]{0:T(128)S(4)} %get-tuple-element.38.slot_ref, bf16[4,256,2048]{2,1,0:T(8,128)(2,1)S(1)} %get-tuple-element.39.x_ref, bf16[2048,512]{1,0:T(8,128)(2,1)S(1)} %get-tuple-element.40.wkv_ref, bf16[2048,512]{1,0:T(8,128)(2,1)} %get-tuple-element.41.wq_hbm, ...), custom_call_target="tpu_custom_call" | custom-call | tf_op jit(solution)/shard_map/cond/branch_1_fun/pallas_call | solution.py:482
  38.1 1.0 %copy.13 = bf16[4,256,512]{2,1,0:T(8,128)(2,1)} copy(bf16[4,256,512]{2,1,0:T(8,128)(2,1)S(1)} %get-tuple-element.50) | data formatting | bytes 2097152
Async XLA Ops:
  0.0 2.3 %copy-start = (s32[4,4,32]{2,1,0:T(4,128)S(1)}, s32[4,4,32]{2,1,0:T(4,128)}, u32[]{:S(2)}) copy-start(s32[4,4,32]{2,1,0:T(4,128)} %param.14) | copy-start | bytes 6148
